TPU v7x, 256 devices: a whole 4x4x8 slice. The times are simulated.
256 devices in a mesh: sp: 16 (over y, x), tp: 16 (over z, core).
Axes of the slice: x: 4, y: 4, z: 8, core: 2. Of those that a mesh axis runs over, the one named last changes fastest.
Arguments:
- residual: bfloat16 [4096, 2048], P(('sp', 'tp')), may hold values from -6 to 6
- mixer_in: bfloat16 [4096, 2048], P('sp', 'tp'), may hold values from -6 to 6
- doc_ids: int32 [4096], P('sp'), may hold values from 0 to 3, never falling along the last dimension, each value on 1 to 1536 neighbouring positions
- lam_re: float32 [128, 64], P('tp'), may hold values from -1 to 0, as said below
- lam_im: float32 [128, 64], P('tp'), may hold values from 0 to 256
- log_step: float32 [128], P('tp'), may hold values from -3 to -2
- log_keep: float32 [4096, 128], P('sp', 'tp'), may hold values from -1.5 to 0, as said below
- in_re: float32 [128, 64, 16], P('tp'), may hold values from -1 to 1
- in_im: float32 [128, 64, 16], P('tp'), may hold values from -1 to 1
- out_re: float32 [128, 16, 64], P('tp'), may hold values from -0.5 to 0.5
- out_im: float32 [128, 16, 64], P('tp'), may hold values from -0.5 to 0.5
- skip_gain: float32 [2048], P('tp'), may hold values from -4 to 4
- w_val: bfloat16 [2048, 2048], P('tp'), may hold values from -0.125 to 0.125
- w_gate: bfloat16 [2048, 2048], P('tp'), may hold values from -0.125 to 0.125
- norm_gain: float32 [2048], replicated, may hold values from 0.1 to 1.9
- route_ids: int32 [4096, 2], P('sp'), may hold values from 0 to 15, all different within a row; in each aligned block of 16 rows (0 to 15, 16 to 31, ...) at most 2 rows name the same one
- route_wts: float32 [4096, 2], P('sp'), may hold values from 0.2 to 1.5
- exp_gate: bfloat16 [16, 2048, 4096], P('sp', None, 'tp'), may hold values from -0.125 to 0.125
- exp_up: bfloat16 [16, 2048, 4096], P('sp', None, 'tp'), may hold values from -0.125 to 0.125
- exp_down: bfloat16 [16, 4096, 2048], P('sp', 'tp'), may hold values from -0.09375 to 0.09375
- shared_gate: bfloat16 [2048, 512], replicated, may hold values from -0.125 to 0.125
- shared_up: bfloat16 [2048, 512], replicated, may hold values from -0.125 to 0.125
- shared_down: bfloat16 [512, 2048], replicated, may hold values from -0.25 to 0.25
Outputs:
- mixed: bfloat16 [4096, 2048], P(('sp', 'tp'))
Inputs may be any that keep to these rules, and one draw needn't show every extreme that they name: `doc_ids`: document numbers start at 0 and never fall; each document has 1 to 1536 positions. `route_ids`: in each aligned block of 16 positions (the positions of one device after the mixer), no expert is named more than 2 times, and some block names one expert exactly 2 times; a position names 2 different experts. `lam_re`: Negative. `log_keep`: never positive.
All inputs are finite; a program needn't handle non-finite values.
Results may differ from a plain program's by a relative error of at most 0.017.
Values may be sent and summed in bfloat16 or wider, within the bound.
No kernel may reach another device: no remote copies, remote signals or barrier semaphores. Data moves between devices by JAX's collectives and lax.ppermute only.
A program may use at most 64 MiB of HBM per device.

v0:
```python
import jax
import jax.numpy as jnp
from jax import lax
from jax.experimental import pallas as pl
from jax.experimental.pallas import tpu as pltpu
from jax.sharding import Mesh, PartitionSpec as P

EPSILON = 1e-06
SP = ("y", "x")
TP = ("z", "core")
STEPS = 32
CHUNKS = 8
LANES = 128
F32 = jnp.float32
BF16 = jnp.bfloat16


def halves(x):
    high = x.astype(BF16)
    return high, (x - high.astype(F32)).astype(BF16)


def dot_nt(a, b):
    return lax.dot_general(a, b, (((1,), (1,)), ((), ())), preferred_element_type=F32)


def block_rows(parts, group_states):
    groups, states = parts.shape
    tiled = jnp.concatenate([parts] * groups, axis=1)
    lane_group = lax.broadcasted_iota(jnp.int32, tiled.shape, 1) // states
    row = lax.broadcasted_iota(jnp.int32, tiled.shape, 0)
    return jnp.sum(jnp.where(lane_group == row, tiled, 0.0), axis=0, keepdims=True)


def decay_rows(lam_re, lam_im, log_step):
    time_step = jnp.exp(log_step)
    magnitude = jnp.exp(lam_re * time_step)
    angle = lam_im * time_step
    return magnitude * jnp.cos(angle), magnitude * jnp.sin(angle)


def squared(re, im, times):
    for _ in range(times):
        re, im = re * re - im * im, 2.0 * re * im
    return re, im


def store_lanes(ref, x):
    for i in range(ref.shape[0]):
        ref[i] = x[:, i * LANES : (i + 1) * LANES]


def strided(ref, j):
    at = pl.ds(j, CHUNKS, stride=STEPS)
    return jnp.concatenate([ref[i, at, :] for i in range(ref.shape[0])], axis=1)


def drive_kernel(
    u_ref, keep_ref, docs_ref, lam_re_ref, lam_im_ref, step_ref, in_re_ref, in_im_ref,
    send_ref, finals_ref, dre_ref, dim_ref, kx_ref, a_ref,
):
    lam_re, lam_im = lam_re_ref[...], lam_im_ref[...]
    groups, states = lam_re.shape
    width = groups * states
    dec_re, dec_im = decay_rows(lam_re, lam_im, step_ref[...])
    denom = lam_re * lam_re + lam_im * lam_im
    less = dec_re - 1.0
    quot_re = block_rows((less * lam_re + dec_im * lam_im) / denom, states)
    quot_im = block_rows((dec_im * lam_re - less * lam_im) / denom, states)
    a_re, a_im = block_rows(dec_re, states), block_rows(dec_im, states)
    a_ref[0:1, :], a_ref[1:2, :] = a_re, a_im
    u = u_ref[...]
    rows, channels = u.shape
    per_group = channels // groups
    row_group = lax.broadcasted_iota(jnp.int32, (width, channels), 0) // states
    lane_group = lax.broadcasted_iota(jnp.int32, (width, channels), 1) // per_group
    own = row_group == lane_group

    def spread(ref):
        tiled = jnp.where(own, jnp.concatenate([ref[...]] * groups, axis=1), 0.0)
        high, low = halves(tiled)
        return dot_nt(u, high) + dot_nt(u, low)

    raw_re, raw_im = spread(in_re_ref), spread(in_im_ref)
    store_lanes(dre_ref, quot_re * raw_re - quot_im * raw_im)
    store_lanes(dim_ref, quot_re * raw_im + quot_im * raw_re)
    expand = (
        lax.broadcasted_iota(jnp.int32, (groups, width), 1) // states
        == lax.broadcasted_iota(jnp.int32, (groups, width), 0)
    ).astype(F32)
    kept_wide = jnp.dot(
        keep_ref[...], expand, precision=lax.Precision.HIGHEST, preferred_element_type=F32
    )
    store_lanes(kx_ref, kept_wide)
    wide = (CHUNKS, width)
    ar, ai = jnp.broadcast_to(a_re, wide), jnp.broadcast_to(a_im, wide)
    s_re, s_im = jnp.zeros(wide, F32), jnp.zeros(wide, F32)
    total = jnp.ones(wide, F32)
    for j in range(STEPS):
        k = strided(kx_ref, j)
        s_re, s_im = (
            k * (ar * s_re - ai * s_im) + strided(dre_ref, j),
            k * (ar * s_im + ai * s_re) + strided(dim_ref, j),
        )
        total = total * k
    finals_ref[0], finals_ref[1], finals_ref[2] = s_re, s_im, total
    b_re, b_im = squared(a_re, a_im, 5)
    c_re, c_im, kept = s_re[0:1], s_im[0:1], total[0:1]
    for c in range(1, CHUNKS):
        k = total[c : c + 1]
        c_re, c_im = (
            k * (b_re * c_re - b_im * c_im) + s_re[c : c + 1],
            k * (b_re * c_im + b_im * c_re) + s_im[c : c + 1],
        )
        kept = kept * k
    packed = jnp.concatenate(
        [c_re, c_im, kept, jnp.broadcast_to(docs_ref[...], (1, width))], axis=0
    )
    send_ref[...] = jnp.broadcast_to(packed[None], send_ref.shape)


def readout_kernel(
    place_ref, got_ref, finals_ref, dre_ref, dim_ref, kx_ref, a_ref, u_ref, out_re_ref, out_im_ref,
    skip_ref, own_ref, other_ref, sre_ref, sim_ref,
):
    position, core = place_ref[0], place_ref[1]
    devices = got_ref.shape[0]
    width = a_ref.shape[1]
    a_re, a_im = a_ref[0:1, :], a_ref[1:2, :]
    b_re, b_im = squared(a_re, a_im, 5)
    w_re, w_im = squared(b_re, b_im, 3)
    c_re, c_im = jnp.zeros((1, width), F32), jnp.zeros((1, width), F32)
    closing = jnp.full((1, width), -1.0, F32)
    for i in range(devices):
        docs = got_ref[i, 3:4, :]
        last = jnp.floor(docs * 0.125)
        first = docs - 8.0 * last
        before = jnp.int32(i) < position
        here = jnp.int32(i) <= position
        linked = jnp.where(first == closing, 1.0, 0.0)
        c_re = jnp.where(here, linked * c_re, c_re)
        c_im = jnp.where(here, linked * c_im, c_im)
        k = got_ref[i, 2:3, :]
        n_re = k * (w_re * c_re - w_im * c_im) + got_ref[i, 0:1, :]
        n_im = k * (w_re * c_im + w_im * c_re) + got_ref[i, 1:2, :]
        c_re, c_im = jnp.where(before, n_re, c_re), jnp.where(before, n_im, c_im)
        closing = last
    heads_re, heads_im = [c_re], [c_im]
    for c in range(CHUNKS - 1):
        k = finals_ref[2, c : c + 1, :]
        c_re, c_im = (
            k * (b_re * c_re - b_im * c_im) + finals_ref[0, c : c + 1, :],
            k * (b_re * c_im + b_im * c_re) + finals_ref[1, c : c + 1, :],
        )
        heads_re.append(c_re)
        heads_im.append(c_im)
    s_re, s_im = jnp.concatenate(heads_re, axis=0), jnp.concatenate(heads_im, axis=0)
    wide = (CHUNKS, width)
    ar, ai = jnp.broadcast_to(a_re, wide), jnp.broadcast_to(a_im, wide)
    for j in range(STEPS):
        k = strided(kx_ref, j)
        s_re, s_im = (
            k * (ar * s_re - ai * s_im) + strided(dre_ref, j),
            k * (ar * s_im + ai * s_re) + strided(dim_ref, j),
        )
        for i in range(width // LANES):
            at = pl.ds(j, CHUNKS, stride=STEPS)
            sre_ref[i, at, :] = s_re[:, i * LANES : (i + 1) * LANES]
            sim_ref[i, at, :] = s_im[:, i * LANES : (i + 1) * LANES]
    rows, channels = u_ref.shape
    states = out_re_ref.shape[1]
    groups = width // states
    row_group = lax.broadcasted_iota(jnp.int32, (channels, width), 0) // (channels // groups)
    lane_group = lax.broadcasted_iota(jnp.int32, (channels, width), 1) // states
    own = row_group == lane_group

    def gathered(state_ref, ref):
        tiled = jnp.where(own, jnp.concatenate([ref[...]] * groups, axis=1), 0.0)
        high, low = halves(tiled)
        blocks = [state_ref[i] for i in range(width // LANES)]
        s_high, s_low = halves(jnp.concatenate(blocks, axis=1))
        return dot_nt(s_high, high) + dot_nt(s_high, low) + dot_nt(s_low, high)

    readout = gathered(sre_ref, out_re_ref) - gathered(sim_ref, out_im_ref)
    readout = readout + skip_ref[...] * u_ref[...].astype(F32)
    active = jax.nn.gelu(readout)
    tiles = active.reshape(rows // 32, 2, 16, channels)
    even, odd = tiles[:, 0], tiles[:, 1]
    own_ref[...] = jnp.where(core == 0, even, odd).reshape(rows // 2, channels).astype(BF16)
    other_ref[...] = jnp.where(core == 0, odd, even).reshape(rows // 2, channels).astype(BF16)


def state_mixer(
    mixer_in, doc_ids, lam_re, lam_im, log_step, log_keep, in_re, in_im, out_re, out_im, skip_gain
):
    rows, channels = mixer_in.shape
    groups, states = lam_re.shape
    width = groups * states
    previous = jnp.concatenate([doc_ids[:1], doc_ids[:-1]])
    keep = jnp.exp(log_keep) * (doc_ids == previous).astype(F32)[:, None]
    docs = (doc_ids[0] + 8 * doc_ids[-1]).astype(F32).reshape(1, 1)
    devices = lax.axis_size(SP)
    big = jax.ShapeDtypeStruct((width // LANES, rows, LANES), F32)
    send, finals, dre, dim, kx, a_rows = pl.pallas_call(
        drive_kernel,
        out_shape=(
            jax.ShapeDtypeStruct((devices, 4, width), F32),
            jax.ShapeDtypeStruct((3, CHUNKS, width), F32),
            big, big, big,
            jax.ShapeDtypeStruct((2, width), F32),
        ),
        name="drive",
    )(
        mixer_in, keep, docs, lam_re, lam_im, log_step.reshape(groups, 1),
        in_re.reshape(width, -1), in_im.reshape(width, -1),
    )
    got = lax.all_to_all(send, SP, 0, 0, tiled=True)
    place = jnp.stack([lax.axis_index(SP), lax.axis_index("core")]).astype(jnp.int32)
    half = jax.ShapeDtypeStruct((rows // 2, channels), BF16)
    in_vmem = pl.BlockSpec(memory_space=pltpu.VMEM)
    return pl.pallas_call(
        readout_kernel,
        out_shape=(half, half),
        in_specs=[pl.BlockSpec(memory_space=pltpu.SMEM)] + [in_vmem] * 10,
        scratch_shapes=[pltpu.VMEM(big.shape, F32), pltpu.VMEM(big.shape, F32)],
        name="readout",
    )(
        place, got, finals, dre, dim, kx, a_rows, mixer_in,
        out_re.reshape(channels, states), out_im.reshape(channels, states),
        skip_gain.reshape(1, channels),
    )


def dot(a, b):
    return jnp.dot(a, b, preferred_element_type=F32)


def on_device(
    residual, mixer_in, doc_ids, lam_re, lam_im, log_step, log_keep, in_re, in_im, out_re, out_im,
    skip_gain, w_val, w_gate, norm_gain, route_ids, route_wts, exp_gate, exp_up, exp_down,
    shared_gate, shared_up, shared_down,
):
    tok_loc, model_width = residual.shape
    layers = lax.axis_size("z")
    owners = lax.axis_size(SP)
    core = lax.axis_index("core")
    top_k = route_ids.shape[1]
    swap = lambda x: lax.ppermute(x, "core", [(0, 1), (1, 0)])
    pair_val, pair_gate = swap(w_val), swap(w_gate)
    pair_eg, pair_eu, pair_ed = swap(exp_gate[0]), swap(exp_up[0]), swap(exp_down[0])

    act_own, act_other = state_mixer(
        mixer_in, doc_ids, lam_re, lam_im, log_step, log_keep, in_re, in_im, out_re, out_im,
        skip_gain,
    )
    act_pair = swap(act_other)
    value = (dot(act_own, w_val) + dot(act_pair, pair_val)).astype(BF16)
    gate = (dot(act_own, w_gate) + dot(act_pair, pair_gate)).astype(BF16)
    parts = jnp.concatenate([value, gate], axis=1).reshape(layers, tok_loc, 2 * model_width)
    parts = lax.all_to_all(parts, "z", 0, 0, tiled=True)
    projected = jnp.sum(parts.astype(F32), axis=0)
    hidden = residual.astype(F32) + projected[:, :model_width] * jax.nn.sigmoid(
        projected[:, model_width:]
    )
    normed = (
        hidden * lax.rsqrt(jnp.mean(hidden * hidden, axis=-1, keepdims=True) + EPSILON) * norm_gain
    ).astype(BF16)

    tokens = layers * tok_loc
    mine = lambda x: lax.dynamic_index_in_dim(
        x.reshape(layers, 2, tok_loc, top_k), core, 1, keepdims=False
    )
    ids = mine(route_ids).reshape(layers, tok_loc * top_k)
    wts = mine(route_wts).reshape(tokens, top_k)
    same = ids[:, :, None] == ids[:, None, :]
    order = jnp.arange(tok_loc * top_k)
    rank = jnp.sum((same & (order[None, :] < order[:, None])).astype(jnp.int32), axis=-1)
    capacity = tok_loc * top_k // owners
    block = layers * capacity
    slots = ids * block + capacity * jnp.arange(layers, dtype=jnp.int32)[:, None] + rank
    slots = slots.reshape(tokens, top_k)
    hit = slots[:, :, None] == jnp.arange(owners * block, dtype=jnp.int32)[None, None, :]
    picker = jnp.sum(hit.astype(F32), axis=1).astype(BF16)
    weights_high, weights_low = halves(jnp.sum(jnp.where(hit, wts[:, :, None], 0.0), axis=1))

    every = jnp.broadcast_to(normed[None], (layers, tok_loc, model_width))
    every = lax.all_to_all(every, "z", 0, 0, tiled=True).reshape(tokens, model_width)
    shared_inner = (jax.nn.silu(dot(normed, shared_gate)) * dot(normed, shared_up)).astype(BF16)
    base = hidden + dot(shared_inner, shared_down)
    packed = lax.dot_general(
        picker, every, (((0,), (0,)), ((), ())), preferred_element_type=F32
    ).astype(BF16)
    rows = lax.all_to_all(packed.reshape(owners, block, model_width), SP, 0, 0, tiled=True)
    rows = rows.reshape(owners * block, model_width)
    inner_own = (jax.nn.silu(dot(rows, exp_gate[0])) * dot(rows, exp_up[0])).astype(BF16)
    inner_pair = (jax.nn.silu(dot(rows, pair_eg)) * dot(rows, pair_eu)).astype(BF16)
    partial = (dot(inner_own, exp_down[0]) + dot(inner_pair, pair_ed)).astype(BF16)
    back = lax.all_to_all(partial.reshape(owners, block, model_width), SP, 0, 0, tiled=True)
    back = back.reshape(owners * block, model_width)
    routed = (dot(weights_high, back) + dot(weights_low, back)).astype(BF16)
    routed = lax.all_to_all(routed.reshape(layers, tok_loc, model_width), "z", 0, 0, tiled=True)
    return (base + jnp.sum(routed.astype(F32), axis=0)).astype(BF16)


def solution(mesh):
    grid = Mesh(mesh.devices.reshape(4, 4, 8, 2), ("y", "x", "z", "core"))
    return jax.shard_map(
        on_device,
        mesh=grid,
        in_specs=(
            P(SP + TP, None),
            P(SP, TP),
            P(SP),
            P(TP, None),
            P(TP, None),
            P(TP),
            P(SP, TP),
            P(TP, None, None),
            P(TP, None, None),
            P(TP, None, None),
            P(TP, None, None),
            P(TP),
            P(TP, None),
            P(TP, None),
            P(),
            P(SP, None),
            P(SP, None),
            P(SP, None, TP),
            P(SP, None, TP),
            P(SP, TP, None),
            P(),
            P(),
            P(),
        ),
        out_specs=P(SP + TP, None),
        check_vma=False,
    )
```

profile of v0, /device:TPU:1, one launch (start us, length us, event | category | flops | bytes accessed | tf_op | source)
XLA Modules:
  0.0 183.2 jit_solution(16635688162617914085)
XLA Ops:
  2.7 1.5 compare_convert_fusion
  5.0 1.7 copy.62
  6.7 1.7 copy.63
  10.4 5.6 %drive.1 = (f32[16,4,512]{2,1,0:T(4,128)}, f32[3,8,512]{2,1,0:T(8,128)}, f32[4,256,128]{2,1,0:T(8,128)}, f32[4,256,128]{2,1,0:T(8,128)}, f32[4,256,128]{2,1,0:T(8,128)}, /*index=5*/f32[2,512]{1,0:T(2,128)}) custom-call(bf16[256,128]{1,0:T(8,128)(2,1)} %u_ref.3, f32[256,8]{1,0:T(8,128)} %broadcast_multiply_fusion.keep_ref, f32[1,1]{1,0:T(1,128)} %bitcast.2.docs_ref, ...), custom_call_target="tpu_custom_call" | custom-call | tf_op jit(solution)/shard_map/drive/pallas_call | solution.py:204
  16.0 7.6 %all-to-all-start = ((f32[16,4,512]{2,1,0:T(4,128)}), f32[16,4,512]{2,1,0:T(4,128)S(1)}, u32[]{:S(2)}, u32[]{:S(2)}) async-start(f32[16,4,512]{2,1,0:T(4,128)} %get-tuple-element.13), calls=%async_computation | async-start | bytes 262144 | tf_op jit(solution)/shard_map/all_to_all | solution.py:217
  25.3 5.1 %all-to-all-done.got_ref = f32[16,4,512]{2,1,0:T(4,128)S(1)} async-done(((f32[16,4,512]{2,1,0:T(4,128)}), f32[16,4,512]{2,1,0:T(4,128)S(1)}, u32[]{:S(2)}, u32[]{:S(2)}) %all-to-all-start) | async-done | bytes 131104 | tf_op jit(solution)/shard_map/all_to_all | solution.py:217
  31.1 4.2 %readout.1 = (bf16[128,128]{1,0:T(8,128)(2,1)}, bf16[128,128]{1,0:T(8,128)(2,1)}) custom-call(s32[2]{0:T(128)} %pad_add_fusion.place_ref, f32[16,4,512]{2,1,0:T(4,128)} %copy-done.3, f32[3,8,512]{2,1,0:T(8,128)} %get-tuple-element.14.finals_ref, f32[4,256,128]{2,1,0:T(8,128)} %get-tuple-element.15.dre_ref, f32[4,256,128]{2,1,0:T(8,128)} %get-tuple-element.16.dim_ref, ...), custom_call_target="tpu_custom_call" | custom-call | tf_op jit(solution)/shard_map/readout/pallas_call | solution.py:221
  35.4 2.1 %collective-permute-start = (bf16[128,128]{1,0:T(8,128)(2,1)}, bf16[128,128]{1,0:T(8,128)(2,1)S(1)}, u32[]{:S(2)}, u32[]{:S(2)}) collective-permute-start(bf16[128,128]{1,0:T(8,128)(2,1)} %get-tuple-element.20), channel_id=1, source_target_pairs={{0,1},{1,0},{2,3},{3,2},{4,5},{5,4},{6,7},{7,6},{8,9},{9,8},{10,11... | collective-permute-start | bytes 98312 | tf_op jit(solution)/shard_map/ppermute | solution.py:248
  43.3 8.3 %all-to-all-start.1 = ((bf16[8,16,4096]{2,1,0:T(8,128)(2,1)}), bf16[8,16,4096]{2,1,0:T(8,128)(2,1)S(1)}, u32[]{:S(2)}, u32[]{:S(2)}) async-start(bf16[8,16,4096]{2,1,0:T(8,128)(2,1)} %bitcast.74), calls=%async_computation.1 | async-start | bytes 2097152 | tf_op jit(solution)/shard_map/all_to_all | solution.py:260
  51.8 29.2 %all-to-all-done.1 = bf16[8,16,4096]{2,1,0:T(8,128)(2,1)S(1)} async-done(((bf16[8,16,4096]{2,1,0:T(8,128)(2,1)}), bf16[8,16,4096]{2,1,0:T(8,128)(2,1)S(1)}, u32[]{:S(2)}, u32[]{:S(2)}) %all-to-all-start.1) | async-done | bytes 1048608 | tf_op jit(solution)/shard_map/all_to_all | solution.py:260
  82.2 3.5 %all-to-all-start.2 = ((bf16[8,16,2048]{2,1,0:T(8,128)(2,1)}), bf16[8,16,2048]{2,1,0:T(8,128)(2,1)S(1)}, u32[]{:S(2)}, u32[]{:S(2)}) async-start(bf16[8,16,2048]{2,1,0:T(8,128)(2,1)} %broadcast_in_dim.19), calls=%async_computation.2 | async-start | bytes 1048576 | tf_op jit(solution)/shard_map/all_to_all | solution.py:287
  87.1 16.5 %all-to-all-done.2 = bf16[8,16,2048]{2,1,0:T(8,128)(2,1)S(1)} async-done(((bf16[8,16,2048]{2,1,0:T(8,128)(2,1)}), bf16[8,16,2048]{2,1,0:T(8,128)(2,1)S(1)}, u32[]{:S(2)}, u32[]{:S(2)}) %all-to-all-start.2) | async-done | bytes 524320 | tf_op jit(solution)/shard_map/all_to_all | solution.py:287
  103.6 1.5 convolution_convert_fusion
  105.0 3.7 %all-to-all-start.3 = ((bf16[16,16,2048]{2,1,0:T(8,128)(2,1)}), bf16[16,16,2048]{2,1,0:T(8,128)(2,1)S(1)}, u32[]{:S(2)}, u32[]{:S(2)}) async-start(bf16[16,16,2048]{2,1,0:T(8,128)(2,1)} %bitcast.73), calls=%async_computation.3 | async-start | bytes 2097152 | tf_op jit(solution)/shard_map/all_to_all | solution.py:293
  109.8 15.4 %all-to-all-done.3 = bf16[16,16,2048]{2,1,0:T(8,128)(2,1)S(1)} async-done(((bf16[16,16,2048]{2,1,0:T(8,128)(2,1)}), bf16[16,16,2048]{2,1,0:T(8,128)(2,1)S(1)}, u32[]{:S(2)}, u32[]{:S(2)}) %all-to-all-start.3) | async-done | bytes 1048608 | tf_op jit(solution)/shard_map/all_to_all | solution.py:293
  125.2 2.4 %fusion.35 = f32[256,256]{1,0:T(8,128)} fusion(bf16[256,2048]{1,0:T(8,128)(2,1)S(1)} %bitcast.66, bf16[1,2048,256]{2,1,0:T(8,128)(2,1)} %param.40), kind=kOutput, calls=%fused_computation.64 | convolution fusion | flops 268435456 | bytes 2359296 | tf_op jit(solution)/shard_map/dot_general | solution.py:235
  127.6 2.4 %fusion.47 = f32[256,256]{1,0:T(8,128)} fusion(bf16[256,2048]{1,0:T(8,128)(2,1)S(1)} %bitcast.67, bf16[2048,256]{1,0:T(8,128)(2,1)} %collective-permute-done.3), kind=kOutput, calls=%fused_computation.74 | convolution fusion | flops 268435456 | bytes 2359296 | tf_op jit(solution)/shard_map/dot_general | solution.py:235
  129.9 4.2 %fusion.7 = f32[256,2048]{1,0:T(8,128)} fusion(bf16[256,2048]{1,0:T(8,128)(2,1)S(1)} %bitcast.68, f32[256,256]{1,0:T(8,128)} %fusion.35, bf16[1,256,2048]{2,1,0:T(8,128)(2,1)} %param.42, bf16[1,2048,256]{2,1,0:T(8,128)(2,1)} %param.41), kind=kOutput, calls=%fused_computation.15 | convolution fusion | flops 537264128 | bytes 5505024 | tf_op jit(solution)/shard_map/dot_general | solution.py:235
  134.2 4.6 %fusion = bf16[256,2048]{1,0:T(8,128)(2,1)} fusion(f32[256,2048]{1,0:T(8,128)} %fusion.7, bf16[256,2048]{1,0:T(8,128)(2,1)} %collective-permute-done.5, f32[256,256]{1,0:T(8,128)} %fusion.47, bf16[256,2048]{1,0:T(8,128)(2,1)S(1)} %bitcast.69, bf16[2048,256]{1,0:T(8,128)(2,1)} %collective-permute-done.4), kind=kOutput, calls=%fused_computation.2 | convolution fusion | flops 538312704 | bytes 6553600 | tf_op jit(solution)/shard_map/dot_general | solution.py:235
  138.8 20.6 %all_to_all.30 = bf16[16,16,2048]{2,1,0:T(8,128)(2,1)S(1)} all-to-all(bf16[16,16,2048]{2,1,0:T(8,128)(2,1)} %bitcast.72), channel_id=1, replica_groups=mesh['y'=4,'x'=4,'z'=8,'core'=2] {'y','x'}, dimensions={0} | all-to-all | bytes 2097152 | tf_op jit(solution)/shard_map/all_to_all | solution.py:298
  160.8 3.5 %all-to-all-start.5 = ((bf16[8,16,2048]{2,1,0:T(8,128)(2,1)}), bf16[8,16,2048]{2,1,0:T(8,128)(2,1)S(1)}, u32[]{:S(2)}, u32[]{:S(2)}) async-start(bf16[8,16,2048]{2,1,0:T(8,128)(2,1)} %bitcast.20), calls=%async_computation.5 | async-start | bytes 1048576 | tf_op jit(solution)/shard_map/all_to_all | solution.py:301
  164.3 2.0 %fusion.46 = f32[16,512]{1,0:T(8,128)S(1)} fusion(bf16[16,2048]{1,0:T(8,128)(2,1)S(1)} %multiply_convert_fusion.2, bf16[2048,512]{1,0:T(8,128)(2,1)} %param.43), kind=kOutput, calls=%fused_computation.73 | convolution fusion | flops 33554432 | bytes 2195456 | tf_op jit(solution)/shard_map/dot_general | solution.py:235
  166.3 13.9 %all-to-all-done.5 = bf16[8,16,2048]{2,1,0:T(8,128)(2,1)S(1)} async-done(((bf16[8,16,2048]{2,1,0:T(8,128)(2,1)}), bf16[8,16,2048]{2,1,0:T(8,128)(2,1)S(1)}, u32[]{:S(2)}, u32[]{:S(2)}) %all-to-all-start.5) | async-done | bytes 524320 | tf_op jit(solution)/shard_map/all_to_all | solution.py:301
  180.3 3.0 %fusion.5 = bf16[16,2048]{1,0:T(8,128)(2,1)} fusion(f32[16,2048]{1,0:T(8,128)S(1)} %convert_reduce_fusion.1, f32[16,2048]{1,0:T(8,128)S(1)} %get-tuple-element.24, bf16[512,2048]{1,0:T(8,128)(2,1)S(1)} %copy-done, bf16[16,2048]{1,0:T(8,128)(2,1)S(1)} %multiply_convert_fusion.2, bf16[2048,512]{1,0:T(8,128)(2,1)} %param.44, f32[16,512]{1,0:T(8,128)S(1)} %fusion.46), kind=kOutput, calls=%fused_computation.11 | convolution fusion | flops 67256320 | bytes 4620288 | tf_op jit(solution)/shard_map/dot_general | solution.py:235
  (64 shorter events, 17.8 us)
Async XLA Ops:
  0.0 180.3 %copy-start = (bf16[512,2048]{1,0:T(8,128)(2,1)S(1)}, bf16[512,2048]{1,0:T(8,128)(2,1)}, u32[]{:S(2)}) copy-start(bf16[512,2048]{1,0:T(8,128)(2,1)} %param.45) | copy-start | bytes 6291460
  0.0 23.6 %copy-start.1 = (bf16[128,2048]{1,0:T(8,128)(2,1)S(1)}, bf16[128,2048]{1,0:T(8,128)(2,1)}, u32[]{:S(2)}) copy-start(bf16[128,2048]{1,0:T(8,128)(2,1)} %param.35) | copy-start | bytes 1572868
  0.0 24.7 %copy-start.2 = (bf16[128,2048]{1,0:T(8,128)(2,1)S(1)}, bf16[128,2048]{1,0:T(8,128)(2,1)}, u32[]{:S(2)}) copy-start(bf16[128,2048]{1,0:T(8,128)(2,1)} %param.36) | copy-start | bytes 1572868
  16.0 14.5 %all-to-all-start = ((f32[16,4,512]{2,1,0:T(4,128)}), f32[16,4,512]{2,1,0:T(4,128)S(1)}, u32[]{:S(2)}, u32[]{:S(2)}) async-start(f32[16,4,512]{2,1,0:T(4,128)} %get-tuple-element.13), calls=%async_computation | async-start | bytes 262144 | tf_op jit(solution)/shard_map/all_to_all | solution.py:217
  23.6 15.9 %collective-permute-start.1 = (bf16[128,2048]{1,0:T(8,128)(2,1)S(1)}, bf16[128,2048]{1,0:T(8,128)(2,1)}, u32[]{:S(2)}, u32[]{:S(2)}) collective-permute-start(bf16[128,2048]{1,0:T(8,128)(2,1)S(1)} %copy-done.1), channel_id=1, source_target_pairs={{0,1},{1,0},{2,3},{3,2},{4,5},{5,4},{6,7},{7,6},{8,9},{9,8},{10,11... | collective-permute-start | bytes 1572872 | tf_op jit(solution)/shard_map/ppermute | solution.py:248
  24.7 16.2 %collective-permute-start.2 = (bf16[128,2048]{1,0:T(8,128)(2,1)S(1)}, bf16[128,2048]{1,0:T(8,128)(2,1)}, u32[]{:S(2)}, u32[]{:S(2)}) collective-permute-start(bf16[128,2048]{1,0:T(8,128)(2,1)S(1)} %copy-done.2), channel_id=1, source_target_pairs={{0,1},{1,0},{2,3},{3,2},{4,5},{5,4},{6,7},{7,6},{8,9},{9,8},{10,11... | collective-permute-start | bytes 1572872 | tf_op jit(solution)/shard_map/ppermute | solution.py:248
  30.5 0.7 copy-start.3
  35.4 4.2 %collective-permute-start = (bf16[128,128]{1,0:T(8,128)(2,1)}, bf16[128,128]{1,0:T(8,128)(2,1)S(1)}, u32[]{:S(2)}, u32[]{:S(2)}) collective-permute-start(bf16[128,128]{1,0:T(8,128)(2,1)} %get-tuple-element.20), channel_id=1, source_target_pairs={{0,1},{1,0},{2,3},{3,2},{4,5},{5,4},{6,7},{7,6},{8,9},{9,8},{10,11... | collective-permute-start | bytes 98312 | tf_op jit(solution)/shard_map/ppermute | solution.py:248
  42.2 9.4 %copy-start.6 = (s32[256,2]{0,1:T(2,128)S(1)}, s32[256,2]{0,1:T(2,128)}, u32[]{:S(2)}) copy-start(s32[256,2]{0,1:T(2,128)} %param.38) | copy-start | bytes 6148
  43.3 37.8 %copy-start.4 = (bf16[16,2048]{1,0:T(8,128)(2,1)S(1)}, bf16[16,2048]{1,0:T(8,128)(2,1)}, u32[]{:S(2)}) copy-start(bf16[16,2048]{1,0:T(8,128)(2,1)} %param.23) | copy-start | bytes 196612
  43.3 37.9 %copy-start.5 = (f32[2048]{0:T(1024)S(1)}, f32[2048]{0:T(1024)}, u32[]{:S(2)}) copy-start(f32[2048]{0:T(1024)} %param.37) | copy-start | bytes 24580
  43.3 37.6 %all-to-all-start.1 = ((bf16[8,16,4096]{2,1,0:T(8,128)(2,1)}), bf16[8,16,4096]{2,1,0:T(8,128)(2,1)S(1)}, u32[]{:S(2)}, u32[]{:S(2)}) async-start(bf16[8,16,4096]{2,1,0:T(8,128)(2,1)} %bitcast.74), calls=%async_computation.1 | async-start | bytes 2097152 | tf_op jit(solution)/shard_map/all_to_all | solution.py:260
  51.6 35.1 %copy-start.7 = (f32[256,2]{0,1:T(2,128)S(1)}, f32[256,2]{0,1:T(2,128)}, u32[]{:S(2)}) copy-start(f32[256,2]{0,1:T(2,128)} %param.39) | copy-start | bytes 6148
  82.2 21.4 %all-to-all-start.2 = ((bf16[8,16,2048]{2,1,0:T(8,128)(2,1)}), bf16[8,16,2048]{2,1,0:T(8,128)(2,1)S(1)}, u32[]{:S(2)}, u32[]{:S(2)}) async-start(bf16[8,16,2048]{2,1,0:T(8,128)(2,1)} %broadcast_in_dim.19), calls=%async_computation.2 | async-start | bytes 1048576 | tf_op jit(solution)/shard_map/all_to_all | solution.py:287
  105.0 20.2 %all-to-all-start.3 = ((bf16[16,16,2048]{2,1,0:T(8,128)(2,1)}), bf16[16,16,2048]{2,1,0:T(8,128)(2,1)S(1)}, u32[]{:S(2)}, u32[]{:S(2)}) async-start(bf16[16,16,2048]{2,1,0:T(8,128)(2,1)} %bitcast.73), calls=%async_computation.3 | async-start | bytes 2097152 | tf_op jit(solution)/shard_map/all_to_all | solution.py:293
  108.7 18.9 %collective-permute-start.3 = (bf16[2048,256]{1,0:T(8,128)(2,1)}, bf16[2048,256]{1,0:T(8,128)(2,1)}, u32[]{:S(2)}, u32[]{:S(2)}) collective-permute-start(bf16[2048,256]{1,0:T(8,128)(2,1)} %bitcast.78), channel_id=1, source_target_pairs={{0,1},{1,0},{2,3},{3,2},{4,5},{5,4},{6,7},{7,6},{8,9},{9,8},{10,11... | collective-permute-start | bytes 3145736 | tf_op jit(solution)/shard_map/ppermute | solution.py:248
  109.3 24.9 %collective-permute-start.4 = (bf16[2048,256]{1,0:T(8,128)(2,1)}, bf16[2048,256]{1,0:T(8,128)(2,1)}, u32[]{:S(2)}, u32[]{:S(2)}) collective-permute-start(bf16[2048,256]{1,0:T(8,128)(2,1)} %bitcast.79), channel_id=1, source_target_pairs={{0,1},{1,0},{2,3},{3,2},{4,5},{5,4},{6,7},{7,6},{8,9},{9,8},{10,11... | collective-permute-start | bytes 3145736 | tf_op jit(solution)/shard_map/ppermute | solution.py:248
  109.4 24.8 %collective-permute-start.5 = (bf16[256,2048]{1,0:T(8,128)(2,1)}, bf16[256,2048]{1,0:T(8,128)(2,1)}, u32[]{:S(2)}, u32[]{:S(2)}) collective-permute-start(bf16[256,2048]{1,0:T(8,128)(2,1)} %bitcast.80), channel_id=1, source_target_pairs={{0,1},{1,0},{2,3},{3,2},{4,5},{5,4},{6,7},{7,6},{8,9},{9,8},{10,11... | collective-permute-start | bytes 3145736 | tf_op jit(solution)/shard_map/ppermute | solution.py:248
  160.8 19.4 %all-to-all-start.5 = ((bf16[8,16,2048]{2,1,0:T(8,128)(2,1)}), bf16[8,16,2048]{2,1,0:T(8,128)(2,1)S(1)}, u32[]{:S(2)}, u32[]{:S(2)}) async-start(bf16[8,16,2048]{2,1,0:T(8,128)(2,1)} %bitcast.20), calls=%async_computation.5 | async-start | bytes 1048576 | tf_op jit(solution)/shard_map/all_to_all | solution.py:301
where the time goes:
time: 184 us; the launch traced here: 183 us
  waiting for transfers between devices  80.1 us (44%)
  starting transfers between devices  30.8 us (17%)
  matrix products  26.1 us (14%)
  blocking collectives  20.6 us (11%)
  Pallas kernels  9.82 us (5%)
  local copies, waits for them, and re-layouts  9.34 us (5%)
  other arithmetic  4.85 us (3%)
    all_to_all x1, waiting for transfers between devices, on_device(): parts = lax.all_to_all(parts, 'z', 0, 0, tiled=True)  29.2 us
    dot_general x12, matrix products, dot(): return jnp.dot(a, b, preferred_element_type=F32)  24.6 us
    all_to_all x1, blocking collectives, on_device(): lax.all_to_all(partial.reshape(owners, block, model_width), SP, 0, 0, til...  20.6 us
    all_to_all x1, waiting for transfers between devices, on_device(): lax.all_to_all(every, 'z', 0, 0, tiled=True).reshape(tokens, model_width)  16.5 us
    all_to_all x1, waiting for transfers between devices, on_device(): lax.all_to_all(packed.reshape(owners, block, model_width), SP, 0, 0, tile...  15.4 us
    all_to_all x1, waiting for transfers between devices, on_device(): lax.all_to_all(routed.reshape(layers, tok_loc, model_width), 'z', 0, 0, t...  13.9 us
    all_to_all x1, starting transfers between devices, on_device(): parts = lax.all_to_all(parts, 'z', 0, 0, tiled=True)  8.31 us
    all_to_all x1, starting transfers between devices, state_mixer(): got = lax.all_to_all(send, SP, 0, 0, tiled=True)  7.58 us
  transfers between devices with their start and end apart: 11, of which 5 were waited for; matrix products, arithmetic and copies ran while one was open for 9% of the time, Pallas kernels for 2%

commit v1 on v0

--- a/solution.py
+++ b/solution.py
@@ -20,6 +20,10 @@
     return high, (x - high.astype(F32)).astype(BF16)
 
 
+def dot(a, b):
+    return jnp.dot(a, b, preferred_element_type=F32)
+
+
 def dot_nt(a, b):
     return lax.dot_general(a, b, (((1,), (1,)), ((), ())), preferred_element_type=F32)
 
@@ -53,6 +57,13 @@
 def strided(ref, j):
     at = pl.ds(j, CHUNKS, stride=STEPS)
     return jnp.concatenate([ref[i, at, :] for i in range(ref.shape[0])], axis=1)
+
+
+def group_masked(parts, groups):
+    tiled = jnp.concatenate([parts] * groups, axis=1)
+    row_group = lax.broadcasted_iota(jnp.int32, tiled.shape, 0) // (parts.shape[0] // groups)
+    lane_group = lax.broadcasted_iota(jnp.int32, tiled.shape, 1) // parts.shape[1]
+    return jnp.where(row_group == lane_group, tiled, 0.0)
 
 
 def drive_kernel(
@@ -62,7 +73,13 @@
     lam_re, lam_im = lam_re_ref[...], lam_im_ref[...]
     groups, states = lam_re.shape
     width = groups * states
-    dec_re, dec_im = decay_rows(lam_re, lam_im, step_ref[...])
+    square = (groups, groups)
+    diagonal = lax.broadcasted_iota(jnp.int32, square, 0) == lax.broadcasted_iota(
+        jnp.int32, square, 1
+    )
+    steps = jnp.broadcast_to(step_ref[...], square)
+    log_step = jnp.sum(jnp.where(diagonal, steps, 0.0), axis=1, keepdims=True)
+    dec_re, dec_im = decay_rows(lam_re, lam_im, log_step)
     denom = lam_re * lam_re + lam_im * lam_im
     less = dec_re - 1.0
     quot_re = block_rows((less * lam_re + dec_im * lam_im) / denom, states)
@@ -70,28 +87,32 @@
     a_re, a_im = block_rows(dec_re, states), block_rows(dec_im, states)
     a_ref[0:1, :], a_ref[1:2, :] = a_re, a_im
     u = u_ref[...]
-    rows, channels = u.shape
-    per_group = channels // groups
-    row_group = lax.broadcasted_iota(jnp.int32, (width, channels), 0) // states
-    lane_group = lax.broadcasted_iota(jnp.int32, (width, channels), 1) // per_group
-    own = row_group == lane_group
 
     def spread(ref):
-        tiled = jnp.where(own, jnp.concatenate([ref[...]] * groups, axis=1), 0.0)
-        high, low = halves(tiled)
-        return dot_nt(u, high) + dot_nt(u, low)
+        high, low = halves(group_masked(ref[...], groups))
+        return dot(u, high) + dot(u, low)
 
     raw_re, raw_im = spread(in_re_ref), spread(in_im_ref)
     store_lanes(dre_ref, quot_re * raw_re - quot_im * raw_im)
     store_lanes(dim_ref, quot_re * raw_im + quot_im * raw_re)
+    docs = docs_ref[...].astype(F32)
+    previous = jnp.concatenate([docs[:, :1], docs[:, :-1]], axis=1)
+    keep = jnp.exp(keep_ref[...]) * (docs == previous).astype(F32)
+    high = keep.astype(BF16)
+    rest = keep - high.astype(F32)
+    middle = rest.astype(BF16)
+    low = (rest - middle.astype(F32)).astype(BF16)
+    split = jnp.concatenate(
+        [high.astype(F32), middle.astype(F32), low.astype(F32), jnp.zeros_like(keep)], axis=0
+    ).astype(BF16)
     expand = (
-        lax.broadcasted_iota(jnp.int32, (groups, width), 1) // states
-        == lax.broadcasted_iota(jnp.int32, (groups, width), 0)
-    ).astype(F32)
-    kept_wide = jnp.dot(
-        keep_ref[...], expand, precision=lax.Precision.HIGHEST, preferred_element_type=F32
-    )
-    store_lanes(kx_ref, kept_wide)
+        lax.broadcasted_iota(jnp.int32, (4 * groups, width), 1) // states
+        == lax.broadcasted_iota(jnp.int32, (4 * groups, width), 0) % groups
+    ).astype(BF16)
+    store_lanes(
+        kx_ref,
+        lax.dot_general(split, expand, (((0,), (0,)), ((), ())), preferred_element_type=F32),
+    )
     wide = (CHUNKS, width)
     ar, ai = jnp.broadcast_to(a_re, wide), jnp.broadcast_to(a_im, wide)
     s_re, s_im = jnp.zeros(wide, F32), jnp.zeros(wide, F32)
@@ -113,17 +134,17 @@
             k * (b_re * c_im + b_im * c_re) + s_im[c : c + 1],
         )
         kept = kept * k
-    packed = jnp.concatenate(
-        [c_re, c_im, kept, jnp.broadcast_to(docs_ref[...], (1, width))], axis=0
-    )
+    both = docs[:, :1] + 8.0 * docs[:, -1:]
+    packed = jnp.concatenate([c_re, c_im, kept, jnp.broadcast_to(both, (1, width))], axis=0)
     send_ref[...] = jnp.broadcast_to(packed[None], send_ref.shape)
 
 
 def readout_kernel(
-    place_ref, got_ref, finals_ref, dre_ref, dim_ref, kx_ref, a_ref, u_ref, out_re_ref, out_im_ref,
+    got_ref, finals_ref, dre_ref, dim_ref, kx_ref, a_ref, u_ref, out_re_ref, out_im_ref,
     skip_ref, own_ref, other_ref, sre_ref, sim_ref,
 ):
-    position, core = place_ref[0], place_ref[1]
+    position = lax.axis_index(SP)
+    core = lax.axis_index("core")
     devices = got_ref.shape[0]
     width = a_ref.shape[1]
     a_re, a_im = a_ref[0:1, :], a_ref[1:2, :]
@@ -170,13 +191,9 @@
     rows, channels = u_ref.shape
     states = out_re_ref.shape[1]
     groups = width // states
-    row_group = lax.broadcasted_iota(jnp.int32, (channels, width), 0) // (channels // groups)
-    lane_group = lax.broadcasted_iota(jnp.int32, (channels, width), 1) // states
-    own = row_group == lane_group
 
     def gathered(state_ref, ref):
-        tiled = jnp.where(own, jnp.concatenate([ref[...]] * groups, axis=1), 0.0)
-        high, low = halves(tiled)
+        high, low = halves(group_masked(ref[...], groups))
         blocks = [state_ref[i] for i in range(width // LANES)]
         s_high, s_low = halves(jnp.concatenate(blocks, axis=1))
         return dot_nt(s_high, high) + dot_nt(s_high, low) + dot_nt(s_low, high)
@@ -196,9 +213,6 @@
     rows, channels = mixer_in.shape
     groups, states = lam_re.shape
     width = groups * states
-    previous = jnp.concatenate([doc_ids[:1], doc_ids[:-1]])
-    keep = jnp.exp(log_keep) * (doc_ids == previous).astype(F32)[:, None]
-    docs = (doc_ids[0] + 8 * doc_ids[-1]).astype(F32).reshape(1, 1)
     devices = lax.axis_size(SP)
     big = jax.ShapeDtypeStruct((width // LANES, rows, LANES), F32)
     send, finals, dre, dim, kx, a_rows = pl.pallas_call(
@@ -211,28 +225,39 @@
         ),
         name="drive",
     )(
-        mixer_in, keep, docs, lam_re, lam_im, log_step.reshape(groups, 1),
-        in_re.reshape(width, -1), in_im.reshape(width, -1),
+        mixer_in, log_keep.T, doc_ids.reshape(1, rows), lam_re, lam_im,
+        log_step.reshape(1, groups), jnp.swapaxes(in_re, 1, 2).reshape(channels, states),
+        jnp.swapaxes(in_im, 1, 2).reshape(channels, states),
     )
     got = lax.all_to_all(send, SP, 0, 0, tiled=True)
-    place = jnp.stack([lax.axis_index(SP), lax.axis_index("core")]).astype(jnp.int32)
     half = jax.ShapeDtypeStruct((rows // 2, channels), BF16)
-    in_vmem = pl.BlockSpec(memory_space=pltpu.VMEM)
     return pl.pallas_call(
         readout_kernel,
         out_shape=(half, half),
-        in_specs=[pl.BlockSpec(memory_space=pltpu.SMEM)] + [in_vmem] * 10,
         scratch_shapes=[pltpu.VMEM(big.shape, F32), pltpu.VMEM(big.shape, F32)],
         name="readout",
     )(
-        place, got, finals, dre, dim, kx, a_rows, mixer_in,
+        got, finals, dre, dim, kx, a_rows, mixer_in,
         out_re.reshape(channels, states), out_im.reshape(channels, states),
         skip_gain.reshape(1, channels),
     )
 
 
-def dot(a, b):
-    return jnp.dot(a, b, preferred_element_type=F32)
+def gated_kernel(own_ref, pair_ref, wv_ref, wg_ref, pv_ref, pg_ref, out_ref):
+    own, pair = own_ref[...], pair_ref[...]
+    width = wv_ref.shape[1]
+    layers, tok_loc, _ = out_ref.shape
+    value = dot(own, wv_ref[...]) + dot(pair, pv_ref[...])
+    out_ref[:, :, :width] = value.reshape(layers, tok_loc, width).astype(BF16)
+    gate = dot(own, wg_ref[...]) + dot(pair, pg_ref[...])
+    out_ref[:, :, width:] = gate.reshape(layers, tok_loc, width).astype(BF16)
+
+
+def expert_kernel(rows_ref, g_ref, u_ref, d_ref, pg_ref, pu_ref, pd_ref, out_ref):
+    rows = rows_ref[...]
+    inner = (jax.nn.silu(dot(rows, g_ref[...])) * dot(rows, u_ref[...])).astype(BF16)
+    pair = (jax.nn.silu(dot(rows, pg_ref[...])) * dot(rows, pu_ref[...])).astype(BF16)
+    out_ref[...] = (dot(inner, d_ref[...]) + dot(pair, pd_ref[...])).astype(BF16)
 
 
 def on_device(
@@ -254,9 +279,11 @@
         skip_gain,
     )
     act_pair = swap(act_other)
-    value = (dot(act_own, w_val) + dot(act_pair, pair_val)).astype(BF16)
-    gate = (dot(act_own, w_gate) + dot(act_pair, pair_gate)).astype(BF16)
-    parts = jnp.concatenate([value, gate], axis=1).reshape(layers, tok_loc, 2 * model_width)
+    parts = pl.pallas_call(
+        gated_kernel,
+        out_shape=jax.ShapeDtypeStruct((layers, tok_loc, 2 * model_width), BF16),
+        name="gated",
+    )(act_own, act_pair, w_val, w_gate, pair_val, pair_gate)
     parts = lax.all_to_all(parts, "z", 0, 0, tiled=True)
     projected = jnp.sum(parts.astype(F32), axis=0)
     hidden = residual.astype(F32) + projected[:, :model_width] * jax.nn.sigmoid(
@@ -287,14 +314,15 @@
     every = lax.all_to_all(every, "z", 0, 0, tiled=True).reshape(tokens, model_width)
     shared_inner = (jax.nn.silu(dot(normed, shared_gate)) * dot(normed, shared_up)).astype(BF16)
     base = hidden + dot(shared_inner, shared_down)
+    every, base = lax.optimization_barrier((every, base))
     packed = lax.dot_general(
         picker, every, (((0,), (0,)), ((), ())), preferred_element_type=F32
     ).astype(BF16)
     rows = lax.all_to_all(packed.reshape(owners, block, model_width), SP, 0, 0, tiled=True)
     rows = rows.reshape(owners * block, model_width)
-    inner_own = (jax.nn.silu(dot(rows, exp_gate[0])) * dot(rows, exp_up[0])).astype(BF16)
-    inner_pair = (jax.nn.silu(dot(rows, pair_eg)) * dot(rows, pair_eu)).astype(BF16)
-    partial = (dot(inner_own, exp_down[0]) + dot(inner_pair, pair_ed)).astype(BF16)
+    partial = pl.pallas_call(
+        expert_kernel, out_shape=jax.ShapeDtypeStruct(rows.shape, BF16), name="expert"
+    )(rows, exp_gate[0], exp_up[0], exp_down[0], pair_eg, pair_eu, pair_ed)
     back = lax.all_to_all(partial.reshape(owners, block, model_width), SP, 0, 0, tiled=True)
     back = back.reshape(owners * block, model_width)
     routed = (dot(weights_high, back) + dot(weights_low, back)).astype(BF16)

time: 184 us -> 161 us (0.88)
  blocking collectives: 20.6 us -> 49.7 us
  waiting for transfers between devices: 80.1 us -> 57.6 us
  matrix products: 26.1 us -> 6.37 us
  starting transfers between devices: 30.8 us -> 21.9 us
  Pallas kernels: 9.82 us -> 17.7 us
  local copies, waits for them, and re-layouts: 9.34 us -> 3.66 us
  other arithmetic: 4.85 us -> 1.67 us
    all_to_all x0 -> x2, blocking collectives: none -> 29.1 us  [the longest x1 17 us: on_device(): lax.all_to_all(routed.reshape(layers, tok_loc, model_width), 'z', 0, 0, t...]
    dot_general x12 -> x4, matrix products: 24.6 us -> 4.92 us  [dot(): return jnp.dot(a, b, preferred_element_type=F32)]
    all_to_all x2 -> x0, waiting for transfers between devices: 19 us -> none  [the longest x1 13.9 us: on_device(): lax.all_to_all(routed.reshape(layers, tok_loc, model_width), 'z', 0, 0, t...]
    all_to_all x2 -> x0, starting transfers between devices: 11.1 us -> none  [the longest x1 7.58 us: state_mixer(): got = lax.all_to_all(send, SP, 0, 0, tiled=True)]
    pallas_call x1 -> x3, Pallas kernels: 4.24 us -> 13.4 us  [the longest x1 5.95 us: on_device(): pl.pallas_call(expert_kernel, out_shape=jax.ShapeDtypeStruct(rows.shape,...]
    all_to_all x1, waiting for transfers between devices: 16.5 us -> 13.3 us  [on_device(): lax.all_to_all(every, 'z', 0, 0, tiled=True).reshape(tokens, model_width)]
    all_to_all x1, waiting for transfers between devices: 29.2 us -> 26.9 us  [on_device(): parts = lax.all_to_all(parts, 'z', 0, 0, tiled=True)]
    unnamed x18, local copies, waits for them, and re-layouts: 4.05 us -> 1.96 us
  transfers between devices with their start and end apart: 11 -> 9, of which waited for: 5 -> 4; matrix products, arithmetic and copies ran while one was open for 9% -> 5% of each run, Pallas kernels for 2% -> 5%
where the time goes in v1:
time: 161 us; the launch traced here: 159 us
  waiting for transfers between devices  57.6 us (36%)
  blocking collectives  49.7 us (31%)
  starting transfers between devices  21.9 us (14%)
  Pallas kernels  17.7 us (11%)
  matrix products  6.37 us (4%)
  local copies, waits for them, and re-layouts  3.66 us (2%)
  other arithmetic  1.67 us (1%)
    all_to_all x1, waiting for transfers between devices, on_device(): parts = lax.all_to_all(parts, 'z', 0, 0, tiled=True)  26.9 us
    all_to_all x1, blocking collectives, on_device(): lax.all_to_all(partial.reshape(owners, block, model_width), SP, 0, 0, til...  20.6 us
    all_to_all x1, blocking collectives, on_device(): lax.all_to_all(routed.reshape(layers, tok_loc, model_width), 'z', 0, 0, t...  17 us
    all_to_all x1, waiting for transfers between devices, on_device(): lax.all_to_all(packed.reshape(owners, block, model_width), SP, 0, 0, tile...  16.3 us
    all_to_all x1, waiting for transfers between devices, on_device(): lax.all_to_all(every, 'z', 0, 0, tiled=True).reshape(tokens, model_width)  13.3 us
    all_to_all x1, blocking collectives, state_mixer(): got = lax.all_to_all(send, SP, 0, 0, tiled=True)  12.1 us
    all_to_all x1, starting transfers between devices, on_device(): parts = lax.all_to_all(parts, 'z', 0, 0, tiled=True)  8.31 us
    ppermute x6, starting transfers between devices, on_device(): swap = lambda x: lax.ppermute(x, 'core', [(0, 1), (1, 0)])  6.3 us
  transfers between devices with their start and end apart: 9, of which 4 were waited for; matrix products, arithmetic and copies ran while one was open for 5% of the time, Pallas kernels for 5%

profile of v1, /device:TPU:1, one launch (start us, length us, event | category | flops | bytes accessed | tf_op | source)
XLA Modules:
  0.0 158.8 jit_solution(17283083361247662018)
XLA Ops:
  0.0 3.2 %collective-permute-start.1 = (bf16[128,2048]{1,0:T(8,128)(2,1)}, bf16[128,2048]{1,0:T(8,128)(2,1)S(1)}, u32[]{:S(2)}, u32[]{:S(2)}) collective-permute-start(bf16[128,2048]{1,0:T(8,128)(2,1)} %wv_ref.1), channel_id=1, source_target_pairs={{0,1},{1,0},{2,3},{3,2},{4,5},{5,4},{6,7},{7,6},{8,9},{9,8},{10,11... | collective-permute-start | bytes 1572872 | tf_op jit(solution)/shard_map/ppermute | solution.py:273
  3.2 4.3 %drive.1 = (f32[16,4,512]{2,1,0:T(4,128)}, f32[3,8,512]{2,1,0:T(8,128)}, f32[4,256,128]{2,1,0:T(8,128)}, f32[4,256,128]{2,1,0:T(8,128)}, f32[4,256,128]{2,1,0:T(8,128)}, /*index=5*/f32[2,512]{1,0:T(2,128)}) custom-call(bf16[256,128]{1,0:T(8,128)(2,1)} %u_ref.3, f32[8,256]{1,0:T(8,128)} %bitcast.65, s32[1,256]{1,0:T(1,128)} %bitcast.66, f32[8,64]{1,0:T(8,128)} %lam_re_ref.1, ...), custom_call_target="tpu_custom_call" | custom-call | tf_op jit(solution)/shard_map/drive/pallas_call | solution.py:218
  7.5 12.1 %all_to_all.30.got_ref = f32[16,4,512]{2,1,0:T(4,128)} all-to-all(f32[16,4,512]{2,1,0:T(4,128)} %get-tuple-element.15), channel_id=1, replica_groups=mesh['y'=4,'x'=4,'z'=8,'core'=2] {'y','x'}, dimensions={0} | all-to-all | bytes 262144 | tf_op jit(solution)/shard_map/all_to_all | solution.py:232
  19.6 4.2 %readout.1 = (bf16[128,128]{1,0:T(8,128)(2,1)}, bf16[128,128]{1,0:T(8,128)(2,1)}) custom-call(f32[16,4,512]{2,1,0:T(4,128)} %all_to_all.30.got_ref, f32[3,8,512]{2,1,0:T(8,128)} %get-tuple-element.16.finals_ref, f32[4,256,128]{2,1,0:T(8,128)} %get-tuple-element.17.dre_ref, f32[4,256,128]{2,1,0:T(8,128)} %get-tuple-element.18.dim_ref, ...), custom_call_target="tpu_custom_call" | custom-call | tf_op jit(solution)/shard_map/readout/pallas_call | solution.py:234
  23.8 2.0 %collective-permute-start = (bf16[128,128]{1,0:T(8,128)(2,1)}, bf16[128,128]{1,0:T(8,128)(2,1)S(1)}, u32[]{:S(2)}, u32[]{:S(2)}) collective-permute-start(bf16[128,128]{1,0:T(8,128)(2,1)} %get-tuple-element.22), channel_id=1, source_target_pairs={{0,1},{1,0},{2,3},{3,2},{4,5},{5,4},{6,7},{7,6},{8,9},{9,8},{10,11... | collective-permute-start | bytes 98312 | tf_op jit(solution)/shard_map/ppermute | solution.py:273
  25.7 1.1 collective-permute-done.pair_ref
  26.8 0.6 copy-done.5
  27.8 3.3 %gated.1 = bf16[8,16,4096]{2,1,0:T(8,128)(2,1)} custom-call(bf16[128,128]{1,0:T(8,128)(2,1)} %get-tuple-element.21.own_ref, bf16[128,128]{1,0:T(8,128)(2,1)} %copy-done.5, bf16[128,2048]{1,0:T(8,128)(2,1)} %wv_ref.1, bf16[128,2048]{1,0:T(8,128)(2,1)} %wg_ref.1, bf16[128,2048]{1,0:T(8,128)(2,1)} %copy-done.2, bf16[128,2048]{1,0:T(8,128)(2,1)} %copy-done.3), custom_call_target="tpu_custom_call" | custom-call | tf_op jit(solution)/shard_map/gated/pallas_call | solution.py:282
  31.1 8.3 %all-to-all-start.1 = ((bf16[8,16,4096]{2,1,0:T(8,128)(2,1)}), bf16[8,16,4096]{2,1,0:T(8,128)(2,1)S(1)}, u32[]{:S(2)}, u32[]{:S(2)}) async-start(bf16[8,16,4096]{2,1,0:T(8,128)(2,1)} %gated.1), calls=%async_computation.1 | async-start | bytes 2097152 | tf_op jit(solution)/shard_map/all_to_all | solution.py:287
  39.4 0.6 collective-permute-start.3
  41.7 26.9 %all-to-all-done.1 = bf16[8,16,4096]{2,1,0:T(8,128)(2,1)S(1)} async-done(((bf16[8,16,4096]{2,1,0:T(8,128)(2,1)}), bf16[8,16,4096]{2,1,0:T(8,128)(2,1)S(1)}, u32[]{:S(2)}, u32[]{:S(2)}) %all-to-all-start.1) | async-done | bytes 1048608 | tf_op jit(solution)/shard_map/all_to_all | solution.py:287
  69.0 0.8 broadcast_in_dim.16
  69.9 3.5 %all-to-all-start.2 = ((bf16[8,16,2048]{2,1,0:T(8,128)(2,1)}), bf16[8,16,2048]{2,1,0:T(8,128)(2,1)S(1)}, u32[]{:S(2)}, u32[]{:S(2)}) async-start(bf16[8,16,2048]{2,1,0:T(8,128)(2,1)} %broadcast_in_dim.16), calls=%async_computation.2 | async-start | bytes 1048576 | tf_op jit(solution)/shard_map/all_to_all | solution.py:314
  73.7 2.0 %fusion.20 = f32[16,512]{1,0:T(8,128)S(1)} fusion(bf16[16,2048]{1,0:T(8,128)(2,1)S(1)} %multiply_convert_fusion, bf16[2048,512]{1,0:T(8,128)(2,1)} %param.43), kind=kOutput, calls=%fused_computation.41 | convolution fusion | flops 33554432 | bytes 2195456 | tf_op jit(solution)/shard_map/dot_general | solution.py:24
  75.6 2.3 %convolution_add_fusion.1 = f32[16,2048]{1,0:T(8,128)S(1)} fusion(f32[16,2048]{1,0:T(8,128)S(1)} %get-tuple-element.28, bf16[512,2048]{1,0:T(8,128)(2,1)S(1)} %copy-done, bf16[16,2048]{1,0:T(8,128)(2,1)S(1)} %multiply_convert_fusion, bf16[2048,512]{1,0:T(8,128)(2,1)} %param.44, f32[16,512]{1,0:T(8,128)S(1)} %fusion.20), kind=kOutput, calls=%fused_computation.3 | convolution fusion | flops 67190784 | bytes 4554752 | tf_op jit(solution)/shard_map/dot_general | solution.py:24
  78.0 13.3 %all-to-all-done.2 = bf16[8,16,2048]{2,1,0:T(8,128)(2,1)S(1)} async-done(((bf16[8,16,2048]{2,1,0:T(8,128)(2,1)}), bf16[8,16,2048]{2,1,0:T(8,128)(2,1)S(1)}, u32[]{:S(2)}, u32[]{:S(2)}) %all-to-all-start.2) | async-done | bytes 524320 | tf_op jit(solution)/shard_map/all_to_all | solution.py:314
  91.2 1.4 convolution_convert_fusion
  92.7 3.8 %all-to-all-start.3 = ((bf16[16,16,2048]{2,1,0:T(8,128)(2,1)}), bf16[16,16,2048]{2,1,0:T(8,128)(2,1)S(1)}, u32[]{:S(2)}, u32[]{:S(2)}) async-start(bf16[16,16,2048]{2,1,0:T(8,128)(2,1)} %bitcast.13), calls=%async_computation.3 | async-start | bytes 2097152 | tf_op jit(solution)/shard_map/all_to_all | solution.py:321
  96.6 16.3 %all-to-all-done.3 = bf16[16,16,2048]{2,1,0:T(8,128)(2,1)S(1)} async-done(((bf16[16,16,2048]{2,1,0:T(8,128)(2,1)}), bf16[16,16,2048]{2,1,0:T(8,128)(2,1)S(1)}, u32[]{:S(2)}, u32[]{:S(2)}) %all-to-all-start.3) | async-done | bytes 1048608 | tf_op jit(solution)/shard_map/all_to_all | solution.py:321
  112.9 1.0 copy-done.1
  113.8 5.9 %expert.1 = bf16[256,2048]{1,0:T(8,128)(2,1)} custom-call(bf16[256,2048]{1,0:T(8,128)(2,1)} %bitcast.47, bf16[2048,256]{1,0:T(8,128)(2,1)} %bitcast.52, bf16[2048,256]{1,0:T(8,128)(2,1)} %bitcast.54, bf16[256,2048]{1,0:T(8,128)(2,1)} %bitcast.56, bf16[2048,256]{1,0:T(8,128)(2,1)} %collective-permute-done.3.pg_ref, ...), custom_call_target="tpu_custom_call" | custom-call | tf_op jit(solution)/shard_map/expert/pallas_call | solution.py:323
  119.8 20.6 %all_to_all.31 = bf16[16,16,2048]{2,1,0:T(8,128)(2,1)S(1)} all-to-all(bf16[16,16,2048]{2,1,0:T(8,128)(2,1)} %bitcast.48), channel_id=1, replica_groups=mesh['y'=4,'x'=4,'z'=8,'core'=2] {'y','x'}, dimensions={0} | all-to-all | bytes 2097152 | tf_op jit(solution)/shard_map/all_to_all | solution.py:326
  141.1 17.0 %all_to_all.32 = bf16[8,16,2048]{2,1,0:T(8,128)(2,1)S(1)} all-to-all(bf16[8,16,2048]{2,1,0:T(8,128)(2,1)S(1)} %bitcast.50), channel_id=1, replica_groups=mesh['y'=4,'x'=4,'z'=8,'core'=2] {'z'}, dimensions={0} | all-to-all | bytes 1048576 | tf_op jit(solution)/shard_map/all_to_all | solution.py:329
  158.2 0.6 add_convert_fusion
  (49 shorter events, 3.4 us)
Async XLA Ops:
  0.0 75.6 %copy-start = (bf16[512,2048]{1,0:T(8,128)(2,1)S(1)}, bf16[512,2048]{1,0:T(8,128)(2,1)}, u32[]{:S(2)}) copy-start(bf16[512,2048]{1,0:T(8,128)(2,1)} %param.45) | copy-start | bytes 6291460
  0.0 26.8 %collective-permute-start.1 = (bf16[128,2048]{1,0:T(8,128)(2,1)}, bf16[128,2048]{1,0:T(8,128)(2,1)S(1)}, u32[]{:S(2)}, u32[]{:S(2)}) collective-permute-start(bf16[128,2048]{1,0:T(8,128)(2,1)} %wv_ref.1), channel_id=1, source_target_pairs={{0,1},{1,0},{2,3},{3,2},{4,5},{5,4},{6,7},{7,6},{8,9},{9,8},{10,11... | collective-permute-start | bytes 1572872 | tf_op jit(solution)/shard_map/ppermute | solution.py:273
  3.2 23.6 %collective-permute-start.2 = (bf16[128,2048]{1,0:T(8,128)(2,1)}, bf16[128,2048]{1,0:T(8,128)(2,1)S(1)}, u32[]{:S(2)}, u32[]{:S(2)}) collective-permute-start(bf16[128,2048]{1,0:T(8,128)(2,1)} %wg_ref.1), channel_id=1, source_target_pairs={{0,1},{1,0},{2,3},{3,2},{4,5},{5,4},{6,7},{7,6},{8,9},{9,8},{10,11... | collective-permute-start | bytes 1572872 | tf_op jit(solution)/shard_map/ppermute | solution.py:273
  23.8 3.0 %collective-permute-start = (bf16[128,128]{1,0:T(8,128)(2,1)}, bf16[128,128]{1,0:T(8,128)(2,1)S(1)}, u32[]{:S(2)}, u32[]{:S(2)}) collective-permute-start(bf16[128,128]{1,0:T(8,128)(2,1)} %get-tuple-element.22), channel_id=1, source_target_pairs={{0,1},{1,0},{2,3},{3,2},{4,5},{5,4},{6,7},{7,6},{8,9},{9,8},{10,11... | collective-permute-start | bytes 98312 | tf_op jit(solution)/shard_map/ppermute | solution.py:273
  26.8 0.6 copy-start.5
  26.8 0.8 copy-start.2
  26.8 1.0 copy-start.3
  27.8 12.7 %copy-start.7 = (f32[256,2]{0,1:T(2,128)S(1)}, f32[256,2]{0,1:T(2,128)}, u32[]{:S(2)}) copy-start(f32[256,2]{0,1:T(2,128)} %param.39) | copy-start | bytes 6148
  27.8 12.9 %copy-start.8 = (s32[256,2]{0,1:T(2,128)S(1)}, s32[256,2]{0,1:T(2,128)}, u32[]{:S(2)}) copy-start(s32[256,2]{0,1:T(2,128)} %param.38) | copy-start | bytes 6148
  31.1 37.7 %copy-start.4 = (bf16[16,2048]{1,0:T(8,128)(2,1)S(1)}, bf16[16,2048]{1,0:T(8,128)(2,1)}, u32[]{:S(2)}) copy-start(bf16[16,2048]{1,0:T(8,128)(2,1)} %param.23) | copy-start | bytes 196612
  31.1 37.9 %copy-start.6 = (f32[2048]{0:T(1024)S(1)}, f32[2048]{0:T(1024)}, u32[]{:S(2)}) copy-start(f32[2048]{0:T(1024)} %param.37) | copy-start | bytes 24580
  31.1 37.6 %all-to-all-start.1 = ((bf16[8,16,4096]{2,1,0:T(8,128)(2,1)}), bf16[8,16,4096]{2,1,0:T(8,128)(2,1)S(1)}, u32[]{:S(2)}, u32[]{:S(2)}) async-start(bf16[8,16,4096]{2,1,0:T(8,128)(2,1)} %gated.1), calls=%async_computation.1 | async-start | bytes 2097152 | tf_op jit(solution)/shard_map/all_to_all | solution.py:287
  39.4 57.2 %collective-permute-start.3 = (bf16[2048,256]{1,0:T(8,128)(2,1)}, bf16[2048,256]{1,0:T(8,128)(2,1)}, u32[]{:S(2)}, u32[]{:S(2)}) collective-permute-start(bf16[2048,256]{1,0:T(8,128)(2,1)} %bitcast.51), channel_id=1, source_target_pairs={{0,1},{1,0},{2,3},{3,2},{4,5},{5,4},{6,7},{7,6},{8,9},{9,8},{10,11... | collective-permute-start | bytes 3145736 | tf_op jit(solution)/shard_map/ppermute | solution.py:273
  40.0 56.5 %collective-permute-start.4 = (bf16[2048,256]{1,0:T(8,128)(2,1)}, bf16[2048,256]{1,0:T(8,128)(2,1)}, u32[]{:S(2)}, u32[]{:S(2)}) collective-permute-start(bf16[2048,256]{1,0:T(8,128)(2,1)} %bitcast.53), channel_id=1, source_target_pairs={{0,1},{1,0},{2,3},{3,2},{4,5},{5,4},{6,7},{7,6},{8,9},{9,8},{10,11... | collective-permute-start | bytes 3145736 | tf_op jit(solution)/shard_map/ppermute | solution.py:273
  40.1 56.5 %collective-permute-start.5 = (bf16[256,2048]{1,0:T(8,128)(2,1)}, bf16[256,2048]{1,0:T(8,128)(2,1)}, u32[]{:S(2)}, u32[]{:S(2)}) collective-permute-start(bf16[256,2048]{1,0:T(8,128)(2,1)} %bitcast.55), channel_id=1, source_target_pairs={{0,1},{1,0},{2,3},{3,2},{4,5},{5,4},{6,7},{7,6},{8,9},{9,8},{10,11... | collective-permute-start | bytes 3145736 | tf_op jit(solution)/shard_map/ppermute | solution.py:273
  69.9 21.4 %all-to-all-start.2 = ((bf16[8,16,2048]{2,1,0:T(8,128)(2,1)}), bf16[8,16,2048]{2,1,0:T(8,128)(2,1)S(1)}, u32[]{:S(2)}, u32[]{:S(2)}) async-start(bf16[8,16,2048]{2,1,0:T(8,128)(2,1)} %broadcast_in_dim.16), calls=%async_computation.2 | async-start | bytes 1048576 | tf_op jit(solution)/shard_map/all_to_all | solution.py:314
  92.7 20.2 %all-to-all-start.3 = ((bf16[16,16,2048]{2,1,0:T(8,128)(2,1)}), bf16[16,16,2048]{2,1,0:T(8,128)(2,1)S(1)}, u32[]{:S(2)}, u32[]{:S(2)}) async-start(bf16[16,16,2048]{2,1,0:T(8,128)(2,1)} %bitcast.13), calls=%async_computation.3 | async-start | bytes 2097152 | tf_op jit(solution)/shard_map/all_to_all | solution.py:321
  112.9 1.0 copy-start.1

commit v2 on v1

--- a/solution.py
+++ b/solution.py
@@ -5,9 +5,11 @@
 from jax.experimental.pallas import tpu as pltpu
 from jax.sharding import Mesh, PartitionSpec as P
 
+
 EPSILON = 1e-06
 SP = ("y", "x")
-TP = ("z", "core")
+TP = ("zh", "zl", "core")
+Z = ("zh", "zl")
 STEPS = 32
 CHUNKS = 8
 LANES = 128
@@ -28,7 +30,7 @@
     return lax.dot_general(a, b, (((1,), (1,)), ((), ())), preferred_element_type=F32)
 
 
-def block_rows(parts, group_states):
+def block_rows(parts):
     groups, states = parts.shape
     tiled = jnp.concatenate([parts] * groups, axis=1)
     lane_group = lax.broadcasted_iota(jnp.int32, tiled.shape, 1) // states
@@ -82,9 +84,9 @@
     dec_re, dec_im = decay_rows(lam_re, lam_im, log_step)
     denom = lam_re * lam_re + lam_im * lam_im
     less = dec_re - 1.0
-    quot_re = block_rows((less * lam_re + dec_im * lam_im) / denom, states)
-    quot_im = block_rows((dec_im * lam_re - less * lam_im) / denom, states)
-    a_re, a_im = block_rows(dec_re, states), block_rows(dec_im, states)
+    quot_re = block_rows((less * lam_re + dec_im * lam_im) / denom)
+    quot_im = block_rows((dec_im * lam_re - less * lam_im) / denom)
+    a_re, a_im = block_rows(dec_re), block_rows(dec_im)
     a_ref[0:1, :], a_ref[1:2, :] = a_re, a_im
     u = u_ref[...]
 
@@ -144,7 +146,7 @@
     skip_ref, own_ref, other_ref, sre_ref, sim_ref,
 ):
     position = lax.axis_index(SP)
-    core = lax.axis_index("core")
+    side = lax.axis_index("zl")
     devices = got_ref.shape[0]
     width = a_ref.shape[1]
     a_re, a_im = a_ref[0:1, :], a_ref[1:2, :]
@@ -201,10 +203,10 @@
     readout = gathered(sre_ref, out_re_ref) - gathered(sim_ref, out_im_ref)
     readout = readout + skip_ref[...] * u_ref[...].astype(F32)
     active = jax.nn.gelu(readout)
-    tiles = active.reshape(rows // 32, 2, 16, channels)
+    tiles = active.reshape(rows // 64, 2, 32, channels)
     even, odd = tiles[:, 0], tiles[:, 1]
-    own_ref[...] = jnp.where(core == 0, even, odd).reshape(rows // 2, channels).astype(BF16)
-    other_ref[...] = jnp.where(core == 0, odd, even).reshape(rows // 2, channels).astype(BF16)
+    own_ref[...] = jnp.where(side == 0, even, odd).reshape(rows // 2, channels).astype(BF16)
+    other_ref[...] = jnp.where(side == 0, odd, even).reshape(rows // 2, channels).astype(BF16)
 
 
 def state_mixer(
@@ -243,14 +245,17 @@
     )
 
 
-def gated_kernel(own_ref, pair_ref, wv_ref, wg_ref, pv_ref, pg_ref, out_ref):
+def gated_kernel(own_ref, pair_ref, wv_ref, wg_ref, fv_ref, fg_ref, keep_ref, send_ref):
     own, pair = own_ref[...], pair_ref[...]
     width = wv_ref.shape[1]
-    layers, tok_loc, _ = out_ref.shape
-    value = dot(own, wv_ref[...]) + dot(pair, pv_ref[...])
-    out_ref[:, :, :width] = value.reshape(layers, tok_loc, width).astype(BF16)
-    gate = dot(own, wg_ref[...]) + dot(pair, pg_ref[...])
-    out_ref[:, :, width:] = gate.reshape(layers, tok_loc, width).astype(BF16)
+    near, tok_loc, _ = keep_ref.shape
+    first = lax.axis_index("core") == 0
+    for at, w_ref, f_ref in ((0, wv_ref, fv_ref), (width, wg_ref, fg_ref)):
+        both = dot(own, w_ref[...]) + dot(pair, f_ref[...])
+        both = both.reshape(near, 2, tok_loc, width)
+        even, odd = both[:, 0], both[:, 1]
+        keep_ref[:, :, at : at + width] = jnp.where(first, even, odd).astype(BF16)
+        send_ref[:, :, at : at + width] = jnp.where(first, odd, even).astype(BF16)
 
 
 def expert_kernel(rows_ref, g_ref, u_ref, d_ref, pg_ref, pu_ref, pd_ref, out_ref):
@@ -266,25 +271,31 @@
     shared_gate, shared_up, shared_down,
 ):
     tok_loc, model_width = residual.shape
-    layers = lax.axis_size("z")
+    layers = lax.axis_size(Z)
     owners = lax.axis_size(SP)
     core = lax.axis_index("core")
     top_k = route_ids.shape[1]
     swap = lambda x: lax.ppermute(x, "core", [(0, 1), (1, 0)])
-    pair_val, pair_gate = swap(w_val), swap(w_gate)
+    cross = lambda x: lax.ppermute(x, "zl", [(0, 1), (1, 0)])
+    near = lax.axis_size("zh")
+    far_val, far_gate = cross(w_val), cross(w_gate)
     pair_eg, pair_eu, pair_ed = swap(exp_gate[0]), swap(exp_up[0]), swap(exp_down[0])
 
     act_own, act_other = state_mixer(
         mixer_in, doc_ids, lam_re, lam_im, log_step, log_keep, in_re, in_im, out_re, out_im,
         skip_gain,
     )
-    act_pair = swap(act_other)
-    parts = pl.pallas_call(
+    act_pair = cross(act_other)
+    kept, sent = pl.pallas_call(
         gated_kernel,
-        out_shape=jax.ShapeDtypeStruct((layers, tok_loc, 2 * model_width), BF16),
+        out_shape=(
+            jax.ShapeDtypeStruct((near, tok_loc, 2 * model_width), BF16),
+            jax.ShapeDtypeStruct((near, tok_loc, 2 * model_width), BF16),
+        ),
         name="gated",
-    )(act_own, act_pair, w_val, w_gate, pair_val, pair_gate)
-    parts = lax.all_to_all(parts, "z", 0, 0, tiled=True)
+    )(act_own, act_pair, w_val, w_gate, far_val, far_gate)
+    parts = (kept.astype(F32) + swap(sent).astype(F32)).astype(BF16)
+    parts = lax.all_to_all(parts, "zh", 0, 0, tiled=True)
     projected = jnp.sum(parts.astype(F32), axis=0)
     hidden = residual.astype(F32) + projected[:, :model_width] * jax.nn.sigmoid(
         projected[:, model_width:]
@@ -311,7 +322,7 @@
     weights_high, weights_low = halves(jnp.sum(jnp.where(hit, wts[:, :, None], 0.0), axis=1))
 
     every = jnp.broadcast_to(normed[None], (layers, tok_loc, model_width))
-    every = lax.all_to_all(every, "z", 0, 0, tiled=True).reshape(tokens, model_width)
+    every = lax.all_to_all(every, Z, 0, 0, tiled=True).reshape(tokens, model_width)
     shared_inner = (jax.nn.silu(dot(normed, shared_gate)) * dot(normed, shared_up)).astype(BF16)
     base = hidden + dot(shared_inner, shared_down)
     every, base = lax.optimization_barrier((every, base))
@@ -326,12 +337,12 @@
     back = lax.all_to_all(partial.reshape(owners, block, model_width), SP, 0, 0, tiled=True)
     back = back.reshape(owners * block, model_width)
     routed = (dot(weights_high, back) + dot(weights_low, back)).astype(BF16)
-    routed = lax.all_to_all(routed.reshape(layers, tok_loc, model_width), "z", 0, 0, tiled=True)
+    routed = lax.all_to_all(routed.reshape(layers, tok_loc, model_width), Z, 0, 0, tiled=True)
     return (base + jnp.sum(routed.astype(F32), axis=0)).astype(BF16)
 
 
 def solution(mesh):
-    grid = Mesh(mesh.devices.reshape(4, 4, 8, 2), ("y", "x", "z", "core"))
+    grid = Mesh(mesh.devices.reshape(4, 4, 4, 2, 2), ("y", "x", "zh", "zl", "core"))
     return jax.shard_map(
         on_device,
         mesh=grid,

time: 161 us -> 150 us (0.932)
  waiting for transfers between devices: 57.6 us -> 40.8 us
  starting transfers between devices: 21.9 us -> 25.3 us
  other arithmetic: 1.67 us -> 3.55 us
    all_to_all x2, waiting for transfers between devices: 40.2 us -> 23.4 us  [the longest x1 12.1 us: on_device(): parts = lax.all_to_all(parts, 'zh', 0, 0, tiled=True)]
    ppermute x0 -> x3, starting transfers between devices: none -> 3.92 us  [on_device(): cross = lambda x: lax.ppermute(x, 'zl', [(0, 1), (1, 0)])]
    all_to_all x1, blocking collectives: 20.6 us -> 17.9 us  [on_device(): lax.all_to_all(partial.reshape(owners, block, model_width), SP, 0, 0, til...]
    ppermute x6 -> x4, starting transfers between devices: 6.3 us -> 4.14 us  [on_device(): swap = lambda x: lax.ppermute(x, 'core', [(0, 1), (1, 0)])]
    convert_element_type x0 -> x1, other arithmetic: none -> 1.95 us  [on_device(): parts = (kept.astype(F32) + swap(sent).astype(F32)).astype(BF16)]
    all_to_all x1, blocking collectives: 12.1 us -> 13.7 us  [state_mixer(): got = lax.all_to_all(send, SP, 0, 0, tiled=True)]
  transfers between devices with their start and end apart: 9 -> 10, of which waited for: 4 -> 5; matrix products, arithmetic and copies ran while one was open for 5% -> 7% of each run, Pallas kernels for 5% -> 6%
where the time goes in v2:
time: 150 us; the launch traced here: 147 us
  blocking collectives  49.9 us (33%)
  waiting for transfers between devices  40.8 us (27%)
  starting transfers between devices  25.3 us (17%)
  Pallas kernels  17.7 us (12%)
  matrix products  6.37 us (4%)
  local copies, waits for them, and re-layouts  3.66 us (2%)
  other arithmetic  3.55 us (2%)
    all_to_all x1, blocking collectives, on_device(): lax.all_to_all(routed.reshape(layers, tok_loc, model_width), Z, 0, 0, til...  18.3 us
    all_to_all x1, blocking collectives, on_device(): lax.all_to_all(partial.reshape(owners, block, model_width), SP, 0, 0, til...  17.9 us
    all_to_all x1, waiting for transfers between devices, on_device(): lax.all_to_all(packed.reshape(owners, block, model_width), SP, 0, 0, tile...  14.7 us
    all_to_all x1, blocking collectives, state_mixer(): got = lax.all_to_all(send, SP, 0, 0, tiled=True)  13.7 us
    all_to_all x1, waiting for transfers between devices, on_device(): parts = lax.all_to_all(parts, 'zh', 0, 0, tiled=True)  12.1 us
    all_to_all x1, waiting for transfers between devices, on_device(): lax.all_to_all(every, Z, 0, 0, tiled=True).reshape(tokens, model_width)  11.3 us
    all_to_all x1, starting transfers between devices, on_device(): parts = lax.all_to_all(parts, 'zh', 0, 0, tiled=True)  8.18 us
    pallas_call x1, Pallas kernels, on_device(): pl.pallas_call(expert_kernel, out_shape=jax.ShapeDtypeStruct(rows.shape,...  5.94 us
  transfers between devices with their start and end apart: 10, of which 5 were waited for; matrix products, arithmetic and copies ran while one was open for 7% of the time, Pallas kernels for 6%

profile of v2, /device:TPU:1, one launch (start us, length us, event | category | flops | bytes accessed | tf_op | source)
XLA Modules:
  0.0 147.4 jit_solution(7625791554229150622)
XLA Ops:
  0.0 2.5 %collective-permute-start.1 = (bf16[128,2048]{1,0:T(8,128)(2,1)}, bf16[128,2048]{1,0:T(8,128)(2,1)S(1)}, u32[]{:S(2)}, u32[]{:S(2)}) collective-permute-start(bf16[128,2048]{1,0:T(8,128)(2,1)} %wv_ref.1), channel_id=1, source_target_pairs={{0,2},{2,0},{1,3},{3,1},{4,6},{6,4},{5,7},{7,5},{8,10},{10,8},{9,1... | collective-permute-start | bytes 1572872 | tf_op jit(solution)/shard_map/ppermute | solution.py:279
  2.6 4.3 %drive.1 = (f32[16,4,512]{2,1,0:T(4,128)}, f32[3,8,512]{2,1,0:T(8,128)}, f32[4,256,128]{2,1,0:T(8,128)}, f32[4,256,128]{2,1,0:T(8,128)}, f32[4,256,128]{2,1,0:T(8,128)}, /*index=5*/f32[2,512]{1,0:T(2,128)}) custom-call(bf16[256,128]{1,0:T(8,128)(2,1)} %u_ref.3, f32[8,256]{1,0:T(8,128)} %bitcast.59, s32[1,256]{1,0:T(1,128)} %bitcast.60, f32[8,64]{1,0:T(8,128)} %lam_re_ref.1, ...), custom_call_target="tpu_custom_call" | custom-call | tf_op jit(solution)/shard_map/drive/pallas_call | solution.py:220
  6.8 13.7 %all_to_all.30.got_ref = f32[16,4,512]{2,1,0:T(4,128)} all-to-all(f32[16,4,512]{2,1,0:T(4,128)} %get-tuple-element.17), channel_id=1, replica_groups=mesh['y'=4,'x'=4,'zh'=4,'zl'=2,'core'=2] {'y','x'}, dimensions={0} | all-to-all | bytes 262144 | tf_op jit(solution)/shard_map/all_to_all | solution.py:234
  20.5 4.2 %readout.1 = (bf16[128,128]{1,0:T(8,128)(2,1)}, bf16[128,128]{1,0:T(8,128)(2,1)}) custom-call(f32[16,4,512]{2,1,0:T(4,128)} %all_to_all.30.got_ref, f32[3,8,512]{2,1,0:T(8,128)} %get-tuple-element.18.finals_ref, f32[4,256,128]{2,1,0:T(8,128)} %get-tuple-element.19.dre_ref, f32[4,256,128]{2,1,0:T(8,128)} %get-tuple-element.20.dim_ref, ...), custom_call_target="tpu_custom_call" | custom-call | tf_op jit(solution)/shard_map/readout/pallas_call | solution.py:236
  24.8 1.4 collective-permute-start
  26.1 1.6 %collective-permute-done.pair_ref = bf16[128,128]{1,0:T(8,128)(2,1)S(1)} collective-permute-done((bf16[128,128]{1,0:T(8,128)(2,1)}, bf16[128,128]{1,0:T(8,128)(2,1)S(1)}, u32[]{:S(2)}, u32[]{:S(2)}) %collective-permute-start) | collective-permute-done | bytes 32800 | tf_op jit(solution)/shard_map/ppermute | solution.py:279
  28.7 3.3 %gated.1 = (bf16[4,16,4096]{2,1,0:T(8,128)(2,1)}, bf16[4,16,4096]{2,1,0:T(8,128)(2,1)}) custom-call(bf16[128,128]{1,0:T(8,128)(2,1)} %get-tuple-element.23.own_ref, bf16[128,128]{1,0:T(8,128)(2,1)} %copy-done.5, bf16[128,2048]{1,0:T(8,128)(2,1)} %wv_ref.1, bf16[128,2048]{1,0:T(8,128)(2,1)} %wg_ref.1, bf16[128,2048]{1,0:T(8,128)(2,1)} %copy-done.2, ...), custom_call_target="tpu_custom_call" | custom-call | tf_op jit(solution)/shard_map/gated/pallas_call | solution.py:289
  32.0 3.5 %collective-permute-start.3 = (bf16[4,16,4096]{2,1,0:T(8,128)(2,1)}, bf16[4,16,4096]{2,1,0:T(8,128)(2,1)S(1)}, u32[]{:S(2)}, u32[]{:S(2)}) collective-permute-start(bf16[4,16,4096]{2,1,0:T(8,128)(2,1)} %get-tuple-element.26), channel_id=1, source_target_pairs={{0,1},{1,0},{2,3},{3,2},{4,5},{5,4},{6,7},{7,6},{8,9},{9,8},{10,11... | collective-permute-start | bytes 1572872 | tf_op jit(solution)/shard_map/ppermute | solution.py:278
  36.2 1.0 collective-permute-done.3
  37.2 2.0 %add_convert_fusion = bf16[4,16,4096]{2,1,0:T(8,128)(2,1)} fusion(bf16[4,16,4096]{2,1,0:T(8,128)(2,1)S(1)} %collective-permute-done.3, bf16[4,16,4096]{2,1,0:T(8,128)(2,1)} %get-tuple-element.25), kind=kLoop, calls=%fused_computation.8 | loop fusion | flops 1048576 | bytes 1572864 | tf_op jit(solution)/shard_map/convert_element_type | solution.py:297
  39.2 8.2 %all-to-all-start.1 = ((bf16[4,16,4096]{2,1,0:T(8,128)(2,1)}), bf16[4,16,4096]{2,1,0:T(8,128)(2,1)S(1)}, u32[]{:S(2)}, u32[]{:S(2)}) async-start(bf16[4,16,4096]{2,1,0:T(8,128)(2,1)} %add_convert_fusion), calls=%async_computation.1 | async-start | bytes 1048576 | tf_op jit(solution)/shard_map/all_to_all | solution.py:298
  48.5 12.1 %all-to-all-done.1 = bf16[4,16,4096]{2,1,0:T(8,128)(2,1)S(1)} async-done(((bf16[4,16,4096]{2,1,0:T(8,128)(2,1)}), bf16[4,16,4096]{2,1,0:T(8,128)(2,1)S(1)}, u32[]{:S(2)}, u32[]{:S(2)}) %all-to-all-start.1) | async-done | bytes 524320 | tf_op jit(solution)/shard_map/all_to_all | solution.py:298
  60.9 0.8 broadcast_in_dim.16
  61.8 5.2 %all-to-all-start.2 = ((bf16[8,16,2048]{2,1,0:T(8,128)(2,1)}), bf16[8,16,2048]{2,1,0:T(8,128)(2,1)S(1)}, u32[]{:S(2)}, u32[]{:S(2)}) async-start(bf16[8,16,2048]{2,1,0:T(8,128)(2,1)} %broadcast_in_dim.16), calls=%async_computation.2 | async-start | bytes 1048576 | tf_op jit(solution)/shard_map/all_to_all | solution.py:325
  67.3 2.0 %fusion.20 = f32[16,512]{1,0:T(8,128)S(1)} fusion(bf16[16,2048]{1,0:T(8,128)(2,1)S(1)} %multiply_convert_fusion, bf16[2048,512]{1,0:T(8,128)(2,1)} %param.43), kind=kOutput, calls=%fused_computation.42 | convolution fusion | flops 33554432 | bytes 2195456 | tf_op jit(solution)/shard_map/dot_general | solution.py:26
  69.3 2.3 %convolution_add_fusion.1 = f32[16,2048]{1,0:T(8,128)S(1)} fusion(f32[16,2048]{1,0:T(8,128)S(1)} %get-tuple-element.32, bf16[512,2048]{1,0:T(8,128)(2,1)S(1)} %copy-done, bf16[16,2048]{1,0:T(8,128)(2,1)S(1)} %multiply_convert_fusion, bf16[2048,512]{1,0:T(8,128)(2,1)} %param.44, f32[16,512]{1,0:T(8,128)S(1)} %fusion.20), kind=kOutput, calls=%fused_computation.3 | convolution fusion | flops 67190784 | bytes 4554752 | tf_op jit(solution)/shard_map/dot_general | solution.py:26
  71.6 11.3 %all-to-all-done.2 = bf16[8,16,2048]{2,1,0:T(8,128)(2,1)S(1)} async-done(((bf16[8,16,2048]{2,1,0:T(8,128)(2,1)}), bf16[8,16,2048]{2,1,0:T(8,128)(2,1)S(1)}, u32[]{:S(2)}, u32[]{:S(2)}) %all-to-all-start.2) | async-done | bytes 524320 | tf_op jit(solution)/shard_map/all_to_all | solution.py:325
  82.9 1.4 convolution_convert_fusion
  84.4 3.8 %all-to-all-start.3 = ((bf16[16,16,2048]{2,1,0:T(8,128)(2,1)}), bf16[16,16,2048]{2,1,0:T(8,128)(2,1)S(1)}, u32[]{:S(2)}, u32[]{:S(2)}) async-start(bf16[16,16,2048]{2,1,0:T(8,128)(2,1)} %bitcast.13), calls=%async_computation.3 | async-start | bytes 2097152 | tf_op jit(solution)/shard_map/all_to_all | solution.py:332
  88.2 14.7 %all-to-all-done.3 = bf16[16,16,2048]{2,1,0:T(8,128)(2,1)S(1)} async-done(((bf16[16,16,2048]{2,1,0:T(8,128)(2,1)}), bf16[16,16,2048]{2,1,0:T(8,128)(2,1)S(1)}, u32[]{:S(2)}, u32[]{:S(2)}) %all-to-all-start.3) | async-done | bytes 1048608 | tf_op jit(solution)/shard_map/all_to_all | solution.py:332
  103.0 1.0 copy-done.1
  104.0 5.9 %expert.1 = bf16[256,2048]{1,0:T(8,128)(2,1)} custom-call(bf16[256,2048]{1,0:T(8,128)(2,1)} %bitcast.47, bf16[2048,256]{1,0:T(8,128)(2,1)} %bitcast.15.g_ref, bf16[2048,256]{1,0:T(8,128)(2,1)} %bitcast.16.u_ref, bf16[256,2048]{1,0:T(8,128)(2,1)} %bitcast.17.d_ref, bf16[2048,256]{1,0:T(8,128)(2,1)} %collective-permute-done.4.pg_ref, ...), custom_call_target="tpu_custom_call" | custom-call | tf_op jit(solution)/shard_map/expert/pallas_call | solution.py:334
  109.9 17.9 %all_to_all.31 = bf16[16,16,2048]{2,1,0:T(8,128)(2,1)S(1)} all-to-all(bf16[16,16,2048]{2,1,0:T(8,128)(2,1)} %bitcast.48), channel_id=1, replica_groups=mesh['y'=4,'x'=4,'zh'=4,'zl'=2,'core'=2] {'y','x'}, dimensions={0} | all-to-all | bytes 2097152 | tf_op jit(solution)/shard_map/all_to_all | solution.py:337
  128.4 18.3 %all_to_all.32 = bf16[8,16,2048]{2,1,0:T(8,128)(2,1)S(1)} all-to-all(bf16[8,16,2048]{2,1,0:T(8,128)(2,1)S(1)} %bitcast.50), channel_id=1, replica_groups=mesh['y'=4,'x'=4,'zh'=4,'zl'=2,'core'=2] {'zh','zl'}, dimensions={0} | all-to-all | bytes 1048576 | tf_op jit(solution)/shard_map/all_to_all | solution.py:340
  (52 shorter events, 4.7 us)
Async XLA Ops:
  0.0 69.3 %copy-start = (bf16[512,2048]{1,0:T(8,128)(2,1)S(1)}, bf16[512,2048]{1,0:T(8,128)(2,1)}, u32[]{:S(2)}) copy-start(bf16[512,2048]{1,0:T(8,128)(2,1)} %param.45) | copy-start | bytes 6291460
  0.0 27.7 %collective-permute-start.1 = (bf16[128,2048]{1,0:T(8,128)(2,1)}, bf16[128,2048]{1,0:T(8,128)(2,1)S(1)}, u32[]{:S(2)}, u32[]{:S(2)}) collective-permute-start(bf16[128,2048]{1,0:T(8,128)(2,1)} %wv_ref.1), channel_id=1, source_target_pairs={{0,2},{2,0},{1,3},{3,1},{4,6},{6,4},{5,7},{7,5},{8,10},{10,8},{9,1... | collective-permute-start | bytes 1572872 | tf_op jit(solution)/shard_map/ppermute | solution.py:279
  2.5 25.3 %collective-permute-start.2 = (bf16[128,2048]{1,0:T(8,128)(2,1)}, bf16[128,2048]{1,0:T(8,128)(2,1)S(1)}, u32[]{:S(2)}, u32[]{:S(2)}) collective-permute-start(bf16[128,2048]{1,0:T(8,128)(2,1)} %wg_ref.1), channel_id=1, source_target_pairs={{0,2},{2,0},{1,3},{3,1},{4,6},{6,4},{5,7},{7,5},{8,10},{10,8},{9,1... | collective-permute-start | bytes 1572872 | tf_op jit(solution)/shard_map/ppermute | solution.py:279
  20.5 15.6 %copy-start.7 = (f32[256,2]{0,1:T(2,128)S(1)}, f32[256,2]{0,1:T(2,128)}, u32[]{:S(2)}) copy-start(f32[256,2]{0,1:T(2,128)} %param.39) | copy-start | bytes 6148
  24.8 3.0 %collective-permute-start = (bf16[128,128]{1,0:T(8,128)(2,1)}, bf16[128,128]{1,0:T(8,128)(2,1)S(1)}, u32[]{:S(2)}, u32[]{:S(2)}) collective-permute-start(bf16[128,128]{1,0:T(8,128)(2,1)} %get-tuple-element.24), channel_id=1, source_target_pairs={{0,2},{2,0},{1,3},{3,1},{4,6},{6,4},{5,7},{7,5},{8,10},{10,8},{9,1... | collective-permute-start | bytes 98312 | tf_op jit(solution)/shard_map/ppermute | solution.py:279
  27.7 0.6 copy-start.5
  27.7 0.8 copy-start.2
  27.7 0.9 copy-start.3
  28.7 18.8 %copy-start.8 = (s32[256,2]{0,1:T(2,128)S(1)}, s32[256,2]{0,1:T(2,128)}, u32[]{:S(2)}) copy-start(s32[256,2]{0,1:T(2,128)} %param.38) | copy-start | bytes 6148
  32.0 28.7 %copy-start.4 = (bf16[16,2048]{1,0:T(8,128)(2,1)S(1)}, bf16[16,2048]{1,0:T(8,128)(2,1)}, u32[]{:S(2)}) copy-start(bf16[16,2048]{1,0:T(8,128)(2,1)} %param.23) | copy-start | bytes 196612
  32.0 5.3 %collective-permute-start.3 = (bf16[4,16,4096]{2,1,0:T(8,128)(2,1)}, bf16[4,16,4096]{2,1,0:T(8,128)(2,1)S(1)}, u32[]{:S(2)}, u32[]{:S(2)}) collective-permute-start(bf16[4,16,4096]{2,1,0:T(8,128)(2,1)} %get-tuple-element.26), channel_id=1, source_target_pairs={{0,1},{1,0},{2,3},{3,2},{4,5},{5,4},{6,7},{7,6},{8,9},{9,8},{10,11... | collective-permute-start | bytes 1572872 | tf_op jit(solution)/shard_map/ppermute | solution.py:278
  35.5 52.7 %collective-permute-start.4 = (bf16[2048,256]{1,0:T(8,128)(2,1)}, bf16[2048,256]{1,0:T(8,128)(2,1)}, u32[]{:S(2)}, u32[]{:S(2)}) collective-permute-start(bf16[2048,256]{1,0:T(8,128)(2,1)} %bitcast.15.g_ref), channel_id=1, source_target_pairs={{0,1},{1,0},{2,3},{3,2},{4,5},{5,4},{6,7},{7,6},{8,9},{9,8},{10,11... | collective-permute-start | bytes 3145736 | tf_op jit(solution)/shard_map/ppermute | solution.py:278
  35.6 52.6 %collective-permute-start.5 = (bf16[2048,256]{1,0:T(8,128)(2,1)}, bf16[2048,256]{1,0:T(8,128)(2,1)}, u32[]{:S(2)}, u32[]{:S(2)}) collective-permute-start(bf16[2048,256]{1,0:T(8,128)(2,1)} %bitcast.16.u_ref), channel_id=1, source_target_pairs={{0,1},{1,0},{2,3},{3,2},{4,5},{5,4},{6,7},{7,6},{8,9},{9,8},{10,11... | collective-permute-start | bytes 3145736 | tf_op jit(solution)/shard_map/ppermute | solution.py:278
  36.0 52.2 %collective-permute-start.6 = (bf16[256,2048]{1,0:T(8,128)(2,1)}, bf16[256,2048]{1,0:T(8,128)(2,1)}, u32[]{:S(2)}, u32[]{:S(2)}) collective-permute-start(bf16[256,2048]{1,0:T(8,128)(2,1)} %bitcast.17.d_ref), channel_id=1, source_target_pairs={{0,1},{1,0},{2,3},{3,2},{4,5},{5,4},{6,7},{7,6},{8,9},{9,8},{10,11... | collective-permute-start | bytes 3145736 | tf_op jit(solution)/shard_map/ppermute | solution.py:278
  36.2 24.6 %copy-start.6 = (f32[2048]{0:T(1024)S(1)}, f32[2048]{0:T(1024)}, u32[]{:S(2)}) copy-start(f32[2048]{0:T(1024)} %param.37) | copy-start | bytes 24580
  39.2 21.4 %all-to-all-start.1 = ((bf16[4,16,4096]{2,1,0:T(8,128)(2,1)}), bf16[4,16,4096]{2,1,0:T(8,128)(2,1)S(1)}, u32[]{:S(2)}, u32[]{:S(2)}) async-start(bf16[4,16,4096]{2,1,0:T(8,128)(2,1)} %add_convert_fusion), calls=%async_computation.1 | async-start | bytes 1048576 | tf_op jit(solution)/shard_map/all_to_all | solution.py:298
  61.8 21.2 %all-to-all-start.2 = ((bf16[8,16,2048]{2,1,0:T(8,128)(2,1)}), bf16[8,16,2048]{2,1,0:T(8,128)(2,1)S(1)}, u32[]{:S(2)}, u32[]{:S(2)}) async-start(bf16[8,16,2048]{2,1,0:T(8,128)(2,1)} %broadcast_in_dim.16), calls=%async_computation.2 | async-start | bytes 1048576 | tf_op jit(solution)/shard_map/all_to_all | solution.py:325
  84.4 18.6 %all-to-all-start.3 = ((bf16[16,16,2048]{2,1,0:T(8,128)(2,1)}), bf16[16,16,2048]{2,1,0:T(8,128)(2,1)S(1)}, u32[]{:S(2)}, u32[]{:S(2)}) async-start(bf16[16,16,2048]{2,1,0:T(8,128)(2,1)} %bitcast.13), calls=%async_computation.3 | async-start | bytes 2097152 | tf_op jit(solution)/shard_map/all_to_all | solution.py:332
  103.0 1.0 copy-start.1

commit v3 on v2

--- a/solution.py
+++ b/solution.py
@@ -12,7 +12,8 @@
 Z = ("zh", "zl")
 STEPS = 32
 CHUNKS = 8
-LANES = 128
+BLOCK = 64
+SMALL = pltpu.CompilerParams(vmem_limit_bytes=16 * 2**20)
 F32 = jnp.float32
 BF16 = jnp.bfloat16
 
@@ -20,6 +21,14 @@
 def halves(x):
     high = x.astype(BF16)
     return high, (x - high.astype(F32)).astype(BF16)
+
+
+def in_hbm(x):
+    return pltpu.with_memory_space_constraint(x, pltpu.HBM)
+
+
+def call(kernel, outs, *operands):
+    return pl.pallas_call(kernel, out_shape=outs, compiler_params=SMALL)(*operands)
 
 
 def dot(a, b):
@@ -51,14 +60,16 @@
     return re, im
 
 
-def store_lanes(ref, x):
-    for i in range(ref.shape[0]):
-        ref[i] = x[:, i * LANES : (i + 1) * LANES]
-
-
-def strided(ref, j):
-    at = pl.ds(j, CHUNKS, stride=STEPS)
-    return jnp.concatenate([ref[i, at, :] for i in range(ref.shape[0])], axis=1)
+def interleaved(rows):
+    square = (rows, rows)
+    row = lax.broadcasted_iota(jnp.int32, square, 0)
+    source = (row % CHUNKS) * STEPS + row // CHUNKS
+    found = lax.broadcasted_iota(jnp.int32, square, 1) == source
+    return jnp.where(found, 1.0, 0.0).astype(BF16)
+
+
+def tile(ref, j):
+    return ref[j * CHUNKS : (j + 1) * CHUNKS, :]
 
 
 def group_masked(parts, groups):
@@ -68,9 +79,9 @@
     return jnp.where(row_group == lane_group, tiled, 0.0)
 
 
-def drive_kernel(
+def fill_drive(
     u_ref, keep_ref, docs_ref, lam_re_ref, lam_im_ref, step_ref, in_re_ref, in_im_ref,
-    send_ref, finals_ref, dre_ref, dim_ref, kx_ref, a_ref,
+    dre_ref, dim_ref, kx_ref, mixed_ref, map_ref,
 ):
     lam_re, lam_im = lam_re_ref[...], lam_im_ref[...]
     groups, states = lam_re.shape
@@ -86,17 +97,11 @@
     less = dec_re - 1.0
     quot_re = block_rows((less * lam_re + dec_im * lam_im) / denom)
     quot_im = block_rows((dec_im * lam_re - less * lam_im) / denom)
-    a_re, a_im = block_rows(dec_re), block_rows(dec_im)
-    a_ref[0:1, :], a_ref[1:2, :] = a_re, a_im
     u = u_ref[...]
-
-    def spread(ref):
-        high, low = halves(group_masked(ref[...], groups))
-        return dot(u, high) + dot(u, low)
-
-    raw_re, raw_im = spread(in_re_ref), spread(in_im_ref)
-    store_lanes(dre_ref, quot_re * raw_re - quot_im * raw_im)
-    store_lanes(dim_ref, quot_re * raw_im + quot_im * raw_re)
+    for k, ref in enumerate((in_re_ref, in_im_ref)):
+        map_ref[2 * k], map_ref[2 * k + 1] = halves(group_masked(ref[...], groups))
+    order = interleaved(u.shape[0])
+    mixed_ref[...] = dot(order, u).astype(BF16)
     docs = docs_ref[...].astype(F32)
     previous = jnp.concatenate([docs[:, :1], docs[:, :-1]], axis=1)
     keep = jnp.exp(keep_ref[...]) * (docs == previous).astype(F32)
@@ -111,19 +116,34 @@
         lax.broadcasted_iota(jnp.int32, (4 * groups, width), 1) // states
         == lax.broadcasted_iota(jnp.int32, (4 * groups, width), 0) % groups
     ).astype(BF16)
-    store_lanes(
-        kx_ref,
-        lax.dot_general(split, expand, (((0,), (0,)), ((), ())), preferred_element_type=F32),
-    )
+    split = dot_nt(split, order).astype(BF16)
+    for start in range(0, u.shape[0], BLOCK):
+        at = slice(start, start + BLOCK)
+        part = mixed_ref[at, :]
+        raw_re = dot(part, map_ref[0]) + dot(part, map_ref[1])
+        raw_im = dot(part, map_ref[2]) + dot(part, map_ref[3])
+        dre_ref[at, :] = quot_re * raw_re - quot_im * raw_im
+        dim_ref[at, :] = quot_re * raw_im + quot_im * raw_re
+        kx_ref[at, :] = lax.dot_general(
+            split[:, at], expand, (((0,), (0,)), ((), ())), preferred_element_type=F32
+        )
+    return block_rows(dec_re), block_rows(dec_im), docs
+
+
+def drive_kernel(*refs):
+    inputs, (send_ref, finals_ref), scratch = refs[:8], refs[8:10], refs[10:]
+    dre_ref, dim_ref, kx_ref = scratch[:3]
+    a_re, a_im, docs = fill_drive(*inputs, *scratch)
+    width = a_re.shape[1]
     wide = (CHUNKS, width)
     ar, ai = jnp.broadcast_to(a_re, wide), jnp.broadcast_to(a_im, wide)
     s_re, s_im = jnp.zeros(wide, F32), jnp.zeros(wide, F32)
     total = jnp.ones(wide, F32)
     for j in range(STEPS):
-        k = strided(kx_ref, j)
+        k = tile(kx_ref, j)
         s_re, s_im = (
-            k * (ar * s_re - ai * s_im) + strided(dre_ref, j),
-            k * (ar * s_im + ai * s_re) + strided(dim_ref, j),
+            k * (ar * s_re - ai * s_im) + tile(dre_ref, j),
+            k * (ar * s_im + ai * s_re) + tile(dim_ref, j),
         )
         total = total * k
     finals_ref[0], finals_ref[1], finals_ref[2] = s_re, s_im, total
@@ -141,15 +161,16 @@
     send_ref[...] = jnp.broadcast_to(packed[None], send_ref.shape)
 
 
-def readout_kernel(
-    got_ref, finals_ref, dre_ref, dim_ref, kx_ref, a_ref, u_ref, out_re_ref, out_im_ref,
-    skip_ref, own_ref, other_ref, sre_ref, sim_ref,
-):
+def readout_kernel(*refs):
+    inputs, (got_ref, finals_ref, out_re_ref, out_im_ref, skip_ref) = refs[:8], refs[8:13]
+    own_ref, other_ref, sre_ref, sim_ref, act_ref = refs[13:18]
+    scratch = refs[18:]
+    dre_ref, dim_ref, kx_ref, u_ref, map_ref = scratch
+    a_re, a_im, _ = fill_drive(*inputs, *scratch)
     position = lax.axis_index(SP)
     side = lax.axis_index("zl")
     devices = got_ref.shape[0]
-    width = a_ref.shape[1]
-    a_re, a_im = a_ref[0:1, :], a_ref[1:2, :]
+    width = a_re.shape[1]
     b_re, b_im = squared(a_re, a_im, 5)
     w_re, w_im = squared(b_re, b_im, 3)
     c_re, c_im = jnp.zeros((1, width), F32), jnp.zeros((1, width), F32)
@@ -181,28 +202,34 @@
     wide = (CHUNKS, width)
     ar, ai = jnp.broadcast_to(a_re, wide), jnp.broadcast_to(a_im, wide)
     for j in range(STEPS):
-        k = strided(kx_ref, j)
+        k = tile(kx_ref, j)
         s_re, s_im = (
-            k * (ar * s_re - ai * s_im) + strided(dre_ref, j),
-            k * (ar * s_im + ai * s_re) + strided(dim_ref, j),
-        )
-        for i in range(width // LANES):
-            at = pl.ds(j, CHUNKS, stride=STEPS)
-            sre_ref[i, at, :] = s_re[:, i * LANES : (i + 1) * LANES]
-            sim_ref[i, at, :] = s_im[:, i * LANES : (i + 1) * LANES]
+            k * (ar * s_re - ai * s_im) + tile(dre_ref, j),
+            k * (ar * s_im + ai * s_re) + tile(dim_ref, j),
+        )
+        sre_ref[j * CHUNKS : (j + 1) * CHUNKS, :] = s_re
+        sim_ref[j * CHUNKS : (j + 1) * CHUNKS, :] = s_im
     rows, channels = u_ref.shape
     states = out_re_ref.shape[1]
     groups = width // states
 
-    def gathered(state_ref, ref):
-        high, low = halves(group_masked(ref[...], groups))
-        blocks = [state_ref[i] for i in range(width // LANES)]
-        s_high, s_low = halves(jnp.concatenate(blocks, axis=1))
-        return dot_nt(s_high, high) + dot_nt(s_high, low) + dot_nt(s_low, high)
-
-    readout = gathered(sre_ref, out_re_ref) - gathered(sim_ref, out_im_ref)
-    readout = readout + skip_ref[...] * u_ref[...].astype(F32)
-    active = jax.nn.gelu(readout)
+    for k, ref in enumerate((out_re_ref, out_im_ref)):
+        map_ref[2 * k], map_ref[2 * k + 1] = halves(group_masked(ref[...], groups))
+
+    def gathered(states, k):
+        high, low = halves(states)
+        return (
+            dot_nt(high, map_ref[k]) + dot_nt(high, map_ref[k + 1]) + dot_nt(low, map_ref[k])
+        )
+
+    for start in range(0, rows, BLOCK):
+        at = slice(start, start + BLOCK)
+        readout = gathered(sre_ref[at, :], 0) - gathered(sim_ref[at, :], 2)
+        readout = readout + skip_ref[...] * u_ref[at, :].astype(F32)
+        act_ref[at, :] = jax.nn.gelu(readout).astype(BF16)
+    active = lax.dot_general(
+        interleaved(rows), act_ref[...], (((0,), (0,)), ((), ())), preferred_element_type=F32
+    )
     tiles = active.reshape(rows // 64, 2, 32, channels)
     even, odd = tiles[:, 0], tiles[:, 1]
     own_ref[...] = jnp.where(side == 0, even, odd).reshape(rows // 2, channels).astype(BF16)
@@ -216,32 +243,36 @@
     groups, states = lam_re.shape
     width = groups * states
     devices = lax.axis_size(SP)
-    big = jax.ShapeDtypeStruct((width // LANES, rows, LANES), F32)
-    send, finals, dre, dim, kx, a_rows = pl.pallas_call(
+    inputs = (
+        mixer_in, log_keep.T, doc_ids.reshape(1, rows), lam_re, lam_im,
+        log_step.reshape(1, groups), jnp.swapaxes(in_re, 1, 2).reshape(channels, states),
+        jnp.swapaxes(in_im, 1, 2).reshape(channels, states),
+    )
+    inputs = tuple(map(in_hbm, inputs))
+    big = pltpu.VMEM((rows, width), F32)
+    mixed = pltpu.VMEM((rows, channels), BF16)
+    scratch = [big, big, big, mixed, pltpu.VMEM((4, channels, width), BF16)]
+    send, finals = pl.pallas_call(
         drive_kernel,
         out_shape=(
             jax.ShapeDtypeStruct((devices, 4, width), F32),
             jax.ShapeDtypeStruct((3, CHUNKS, width), F32),
-            big, big, big,
-            jax.ShapeDtypeStruct((2, width), F32),
         ),
+        scratch_shapes=scratch,
         name="drive",
-    )(
-        mixer_in, log_keep.T, doc_ids.reshape(1, rows), lam_re, lam_im,
-        log_step.reshape(1, groups), jnp.swapaxes(in_re, 1, 2).reshape(channels, states),
-        jnp.swapaxes(in_im, 1, 2).reshape(channels, states),
-    )
+        compiler_params=SMALL,
+    )(*inputs)
     got = lax.all_to_all(send, SP, 0, 0, tiled=True)
     half = jax.ShapeDtypeStruct((rows // 2, channels), BF16)
     return pl.pallas_call(
         readout_kernel,
         out_shape=(half, half),
-        scratch_shapes=[pltpu.VMEM(big.shape, F32), pltpu.VMEM(big.shape, F32)],
+        scratch_shapes=[big, big, mixed, *scratch],
         name="readout",
+        compiler_params=SMALL,
     )(
-        got, finals, dre, dim, kx, a_rows, mixer_in,
-        out_re.reshape(channels, states), out_im.reshape(channels, states),
-        skip_gain.reshape(1, channels),
+        *inputs, got, finals, in_hbm(out_re.reshape(channels, states)),
+        in_hbm(out_im.reshape(channels, states)), in_hbm(skip_gain.reshape(1, channels)),
     )
 
 
@@ -256,6 +287,22 @@
         even, odd = both[:, 0], both[:, 1]
         keep_ref[:, :, at : at + width] = jnp.where(first, even, odd).astype(BF16)
         send_ref[:, :, at : at + width] = jnp.where(first, odd, even).astype(BF16)
+
+
+def sum_kernel(kept_ref, got_ref, out_ref):
+    out_ref[...] = (kept_ref[...].astype(F32) + got_ref[...].astype(F32)).astype(BF16)
+
+
+def norm_kernel(parts_ref, res_ref, gain_ref, every_ref, hidden_ref, normed_ref):
+    width = res_ref.shape[1]
+    value = jnp.sum(parts_ref[:, :, :width].astype(F32), axis=0)
+    gate = jnp.sum(parts_ref[:, :, width:].astype(F32), axis=0)
+    hidden = res_ref[...].astype(F32) + value * jax.nn.sigmoid(gate)
+    mean = jnp.mean(hidden * hidden, axis=-1, keepdims=True)
+    normed = (hidden * lax.rsqrt(mean + EPSILON) * gain_ref[...]).astype(BF16)
+    hidden_ref[...] = hidden
+    normed_ref[...] = normed
+    every_ref[...] = jnp.broadcast_to(normed[None], every_ref.shape)
 
 
 def expert_kernel(rows_ref, g_ref, u_ref, d_ref, pg_ref, pu_ref, pd_ref, out_ref):
@@ -279,30 +326,30 @@
     cross = lambda x: lax.ppermute(x, "zl", [(0, 1), (1, 0)])
     near = lax.axis_size("zh")
     far_val, far_gate = cross(w_val), cross(w_gate)
-    pair_eg, pair_eu, pair_ed = swap(exp_gate[0]), swap(exp_up[0]), swap(exp_down[0])
+    gate_w, up_w, down_w = exp_gate[0], exp_up[0], exp_down[0]
+    pair_eg, pair_eu, pair_ed = swap(gate_w), swap(up_w), swap(down_w)
 
     act_own, act_other = state_mixer(
         mixer_in, doc_ids, lam_re, lam_im, log_step, log_keep, in_re, in_im, out_re, out_im,
         skip_gain,
     )
     act_pair = cross(act_other)
-    kept, sent = pl.pallas_call(
-        gated_kernel,
-        out_shape=(
-            jax.ShapeDtypeStruct((near, tok_loc, 2 * model_width), BF16),
-            jax.ShapeDtypeStruct((near, tok_loc, 2 * model_width), BF16),
+    shape = jax.ShapeDtypeStruct((near, tok_loc, 2 * model_width), BF16)
+    kept, sent = call(
+        gated_kernel, (shape, shape),
+        act_own, act_pair, in_hbm(w_val), in_hbm(w_gate), far_val, far_gate,
+    )
+    parts = call(sum_kernel, shape, kept, swap(sent))
+    parts = lax.all_to_all(parts, "zh", 0, 0, tiled=True)
+    every, hidden, normed = call(
+        norm_kernel,
+        (
+            jax.ShapeDtypeStruct((layers, tok_loc, model_width), BF16),
+            jax.ShapeDtypeStruct(residual.shape, F32),
+            jax.ShapeDtypeStruct(residual.shape, BF16),
         ),
-        name="gated",
-    )(act_own, act_pair, w_val, w_gate, far_val, far_gate)
-    parts = (kept.astype(F32) + swap(sent).astype(F32)).astype(BF16)
-    parts = lax.all_to_all(parts, "zh", 0, 0, tiled=True)
-    projected = jnp.sum(parts.astype(F32), axis=0)
-    hidden = residual.astype(F32) + projected[:, :model_width] * jax.nn.sigmoid(
-        projected[:, model_width:]
-    )
-    normed = (
-        hidden * lax.rsqrt(jnp.mean(hidden * hidden, axis=-1, keepdims=True) + EPSILON) * norm_gain
-    ).astype(BF16)
+        parts, residual, norm_gain.reshape(1, model_width),
+    )
 
     tokens = layers * tok_loc
     mine = lambda x: lax.dynamic_index_in_dim(
@@ -321,7 +368,6 @@
     picker = jnp.sum(hit.astype(F32), axis=1).astype(BF16)
     weights_high, weights_low = halves(jnp.sum(jnp.where(hit, wts[:, :, None], 0.0), axis=1))
 
-    every = jnp.broadcast_to(normed[None], (layers, tok_loc, model_width))
     every = lax.all_to_all(every, Z, 0, 0, tiled=True).reshape(tokens, model_width)
     shared_inner = (jax.nn.silu(dot(normed, shared_gate)) * dot(normed, shared_up)).astype(BF16)
     base = hidden + dot(shared_inner, shared_down)
@@ -331,9 +377,13 @@
     ).astype(BF16)
     rows = lax.all_to_all(packed.reshape(owners, block, model_width), SP, 0, 0, tiled=True)
     rows = rows.reshape(owners * block, model_width)
+    operands = (rows, gate_w, up_w, down_w, pair_eg, pair_eu, pair_ed)
     partial = pl.pallas_call(
-        expert_kernel, out_shape=jax.ShapeDtypeStruct(rows.shape, BF16), name="expert"
-    )(rows, exp_gate[0], exp_up[0], exp_down[0], pair_eg, pair_eu, pair_ed)
+        expert_kernel,
+        out_shape=jax.ShapeDtypeStruct(rows.shape, BF16),
+        name="expert",
+        compiler_params=SMALL,
+    )(*operands)
     back = lax.all_to_all(partial.reshape(owners, block, model_width), SP, 0, 0, tiled=True)
     back = back.reshape(owners * block, model_width)
     routed = (dot(weights_high, back) + dot(weights_low, back)).astype(BF16)

time: 150 us -> 145 us (0.967)
  Pallas kernels: 17.7 us -> 14.7 us
  local copies, waits for them, and re-layouts: 3.66 us -> 0.89 us
  other arithmetic: 3.55 us -> 1.29 us
  blocking collectives: 49.9 us -> 51.7 us
    all_to_all x1, blocking collectives: 18.3 us -> 21.1 us  [on_device(): lax.all_to_all(routed.reshape(layers, tok_loc, model_width), Z, 0, 0, til...]
    all_to_all x1, starting transfers between devices: 3.83 us -> 6.41 us  [on_device(): lax.all_to_all(packed.reshape(owners, block, model_width), SP, 0, 0, tile...]
    pallas_call x1, Pallas kernels: 4.27 us -> 1.9 us  [state_mixer(): pl.pallas_call(drive_kernel, out_shape=(jax.ShapeDtypeStruct((devices, 4,...]
    convert_element_type x2 -> x0, other arithmetic: 2.03 us -> none  [the longest x1 1.95 us: on_device(): parts = (kept.astype(F32) + swap(sent).astype(F32)).astype(BF16)]
    unnamed x18 -> x10, local copies, waits for them, and re-layouts: 1.96 us -> 0.02 us
    pallas_call x2 -> x4, Pallas kernels: 7.49 us -> 8.05 us  [the longest x3 4.74 us: call(): pl.pallas_call(kernel, out_shape=outs, compiler_params=SMALL)(*operands)]
  transfers between devices with their start and end apart: 10 -> 10, of which waited for: 5 -> 5; matrix products, arithmetic and copies ran while one was open for 7% -> 5% of each run, Pallas kernels for 6% -> 5%
where the time goes in v3:
time: 145 us; the launch traced here: 144 us
  blocking collectives  51.7 us (36%)
  waiting for transfers between devices  42 us (29%)
  starting transfers between devices  26.6 us (18%)
  Pallas kernels  14.7 us (10%)
  matrix products  6.37 us (4%)
    all_to_all x1, blocking collectives, on_device(): lax.all_to_all(routed.reshape(layers, tok_loc, model_width), Z, 0, 0, til...  21.1 us
    all_to_all x1, blocking collectives, on_device(): lax.all_to_all(partial.reshape(owners, block, model_width), SP, 0, 0, til...  17.3 us
    all_to_all x1, waiting for transfers between devices, on_device(): lax.all_to_all(packed.reshape(owners, block, model_width), SP, 0, 0, tile...  14.7 us
    all_to_all x1, blocking collectives, state_mixer(): got = lax.all_to_all(send, SP, 0, 0, tiled=True)  13.4 us
    all_to_all x1, waiting for transfers between devices, on_device(): parts = lax.all_to_all(parts, 'zh', 0, 0, tiled=True)  12.2 us
    all_to_all x1, waiting for transfers between devices, on_device(): lax.all_to_all(every, Z, 0, 0, tiled=True).reshape(tokens, model_width)  11.3 us
    all_to_all x1, starting transfers between devices, on_device(): parts = lax.all_to_all(parts, 'zh', 0, 0, tiled=True)  8.2 us
    all_to_all x1, starting transfers between devices, on_device(): lax.all_to_all(packed.reshape(owners, block, model_width), SP, 0, 0, tile...  6.41 us
  transfers between devices with their start and end apart: 10, of which 5 were waited for; matrix products, arithmetic and copies ran while one was open for 5% of the time, Pallas kernels for 5%

profile of v3, /device:TPU:1, one launch (start us, length us, event | category | flops | bytes accessed | tf_op | source)
XLA Modules:
  0.0 143.7 jit_solution(3233732956193727733)
XLA Ops:
  0.0 2.5 %collective-permute-start.1 = (bf16[128,2048]{1,0:T(8,128)(2,1)}, bf16[128,2048]{1,0:T(8,128)(2,1)S(1)}, u32[]{:S(2)}, u32[]{:S(2)}) collective-permute-start(bf16[128,2048]{1,0:T(8,128)(2,1)} %wv_ref.1), channel_id=1, source_target_pairs={{0,2},{2,0},{1,3},{3,1},{4,6},{6,4},{5,7},{7,5},{8,10},{10,8},{9,1... | collective-permute-start | bytes 1572872 | tf_op jit(solution)/shard_map/ppermute | solution.py:326
  2.6 1.9 %drive.1 = (f32[16,4,512]{2,1,0:T(4,128)S(1)}, f32[3,8,512]{2,1,0:T(8,128)S(1)}) custom-call(bf16[256,128]{1,0:T(8,128)(2,1)} %refs_0_.3, f32[8,256]{1,0:T(8,128)} %bitcast.63, s32[1,256]{1,0:T(1,128)} %bitcast.66, f32[8,64]{1,0:T(8,128)} %refs_3_.3, f32[8,64]{1,0:T(8,128)} %refs_4_.3, f32[1,8]{1,0:T(1,128)} %bitcast.68, f32[128,64]{1,0:T(8,128)} %bitcast.54, ...), custom_call_target="tpu_custom_call" | custom-call | tf_op jit(solution)/shard_map/drive/pallas_call | solution.py:255
  4.5 13.4 %all_to_all.30.refs_8_ = f32[16,4,512]{2,1,0:T(4,128)S(1)} all-to-all(f32[16,4,512]{2,1,0:T(4,128)S(1)} %get-tuple-element.16), channel_id=1, replica_groups=mesh['y'=4,'x'=4,'zh'=4,'zl'=2,'core'=2] {'y','x'}, dimensions={0} | all-to-all | bytes 262144 | tf_op jit(solution)/shard_map/all_to_all | solution.py:265
  17.8 3.3 %readout.1 = (bf16[128,128]{1,0:T(8,128)(2,1)S(1)}, bf16[128,128]{1,0:T(8,128)(2,1)S(1)}) custom-call(bf16[256,128]{1,0:T(8,128)(2,1)} %refs_0_.3, f32[8,256]{1,0:T(8,128)} %bitcast.64, s32[1,256]{1,0:T(1,128)} %bitcast.67, f32[8,64]{1,0:T(8,128)} %refs_3_.3, f32[8,64]{1,0:T(8,128)} %refs_4_.3, f32[1,8]{1,0:T(1,128)} %bitcast.69, f32[128,64]{1,0:T(8,128)} %bitcast.55, ...), custom_call_target="tpu_custom_call" | custom-call | tf_op jit(solution)/shard_map/readout/pallas_call | solution.py:267
  21.2 1.5 %collective-permute-start = (bf16[128,128]{1,0:T(8,128)(2,1)S(1)}, bf16[128,128]{1,0:T(8,128)(2,1)S(1)}, u32[]{:S(2)}, u32[]{:S(2)}) collective-permute-start(bf16[128,128]{1,0:T(8,128)(2,1)S(1)} %get-tuple-element.19), channel_id=1, source_target_pairs={{0,2},{2,0},{1,3},{3,1},{4,6},{6,4},{5,7},{7,5},{8,10},{10,8},{9,1... | collective-permute-start | bytes 98312 | tf_op jit(solution)/shard_map/ppermute | solution.py:326
  22.6 2.6 %collective-permute-done.pair_ref = bf16[128,128]{1,0:T(8,128)(2,1)S(1)} collective-permute-done((bf16[128,128]{1,0:T(8,128)(2,1)S(1)}, bf16[128,128]{1,0:T(8,128)(2,1)S(1)}, u32[]{:S(2)}, u32[]{:S(2)}) %collective-permute-start) | collective-permute-done | bytes 32800 | tf_op jit(solution)/shard_map/ppermute | solution.py:326
  25.3 2.8 %shard_map.217 = (bf16[4,16,4096]{2,1,0:T(8,128)(2,1)S(1)}, bf16[4,16,4096]{2,1,0:T(8,128)(2,1)}) custom-call(bf16[128,128]{1,0:T(8,128)(2,1)S(1)} %get-tuple-element.18.own_ref, bf16[128,128]{1,0:T(8,128)(2,1)S(1)} %collective-permute-done.pair_ref, bf16[128,2048]{1,0:T(8,128)(2,1)} %wv_ref.1, bf16[128,2048]{1,0:T(8,128)(2,1)} %wg_ref.1, ...), custom_call_target="tpu_custom_call" | custom-call | tf_op jit(solution)/shard_map/pallas_call | solution.py:31
  28.0 2.3 %collective-permute-start.3 = (bf16[4,16,4096]{2,1,0:T(8,128)(2,1)}, bf16[4,16,4096]{2,1,0:T(8,128)(2,1)S(1)}, u32[]{:S(2)}, u32[]{:S(2)}) collective-permute-start(bf16[4,16,4096]{2,1,0:T(8,128)(2,1)} %get-tuple-element.21), channel_id=1, source_target_pairs={{0,1},{1,0},{2,3},{3,2},{4,5},{5,4},{6,7},{7,6},{8,9},{9,8},{10,11... | collective-permute-start | bytes 1572872 | tf_op jit(solution)/shard_map/ppermute | solution.py:325
  30.9 1.2 collective-permute-done.3.got_ref
  32.1 0.9 shard_map.218
  33.1 8.2 %all-to-all-start.1 = ((bf16[4,16,4096]{2,1,0:T(8,128)(2,1)}), bf16[4,16,4096]{2,1,0:T(8,128)(2,1)S(1)}, u32[]{:S(2)}, u32[]{:S(2)}) async-start(bf16[4,16,4096]{2,1,0:T(8,128)(2,1)} %shard_map.218), calls=%async_computation.1 | async-start | bytes 1048576 | tf_op jit(solution)/shard_map/all_to_all | solution.py:343
  42.4 12.2 %all-to-all-done.1.parts_ref = bf16[4,16,4096]{2,1,0:T(8,128)(2,1)S(1)} async-done(((bf16[4,16,4096]{2,1,0:T(8,128)(2,1)}), bf16[4,16,4096]{2,1,0:T(8,128)(2,1)S(1)}, u32[]{:S(2)}, u32[]{:S(2)}) %all-to-all-start.1) | async-done | bytes 524320 | tf_op jit(solution)/shard_map/all_to_all | solution.py:343
  54.6 1.0 shard_map.219
  55.6 5.1 %all-to-all-start.2 = ((bf16[8,16,2048]{2,1,0:T(8,128)(2,1)}), bf16[8,16,2048]{2,1,0:T(8,128)(2,1)S(1)}, u32[]{:S(2)}, u32[]{:S(2)}) async-start(bf16[8,16,2048]{2,1,0:T(8,128)(2,1)} %get-tuple-element.22), calls=%async_computation.2 | async-start | bytes 1048576 | tf_op jit(solution)/shard_map/all_to_all | solution.py:371
  61.0 2.0 %fusion.15 = f32[16,512]{1,0:T(8,128)S(1)} fusion(bf16[16,2048]{1,0:T(8,128)(2,1)S(1)} %get-tuple-element.24, bf16[2048,512]{1,0:T(8,128)(2,1)} %param.43), kind=kOutput, calls=%fused_computation.31 | convolution fusion | flops 33554432 | bytes 2195456 | tf_op jit(solution)/shard_map/dot_general | solution.py:35
  63.0 2.3 %fusion.2 = f32[16,2048]{1,0:T(8,128)S(1)} fusion(bf16[512,2048]{1,0:T(8,128)(2,1)S(1)} %copy-done, bf16[16,2048]{1,0:T(8,128)(2,1)S(1)} %get-tuple-element.24, bf16[2048,512]{1,0:T(8,128)(2,1)} %param.44, f32[16,512]{1,0:T(8,128)S(1)} %fusion.15), kind=kOutput, calls=%fused_computation.5 | convolution fusion | flops 67158016 | bytes 4423680 | tf_op jit(solution)/shard_map/dot_general | solution.py:35
  65.4 11.3 %all-to-all-done.2 = bf16[8,16,2048]{2,1,0:T(8,128)(2,1)S(1)} async-done(((bf16[8,16,2048]{2,1,0:T(8,128)(2,1)}), bf16[8,16,2048]{2,1,0:T(8,128)(2,1)S(1)}, u32[]{:S(2)}, u32[]{:S(2)}) %all-to-all-start.2) | async-done | bytes 524320 | tf_op jit(solution)/shard_map/all_to_all | solution.py:371
  76.7 1.5 %convolution_convert_fusion = bf16[256,2048]{1,0:T(8,128)(2,1)} fusion(bf16[128,2048]{1,0:T(8,128)(2,1)S(1)} %bitcast.52, bf16[128,256]{1,0:T(8,128)(2,1)S(1)} %get-tuple-element.28), kind=kOutput, calls=%fused_computation | convolution fusion | flops 134742016 | bytes 1638400 | tf_op jit(solution)/shard_map/dot_general | solution.py:375
  78.2 6.4 %all-to-all-start.3 = ((bf16[16,16,2048]{2,1,0:T(8,128)(2,1)}), bf16[16,16,2048]{2,1,0:T(8,128)(2,1)S(1)}, u32[]{:S(2)}, u32[]{:S(2)}) async-start(bf16[16,16,2048]{2,1,0:T(8,128)(2,1)} %bitcast.51), calls=%async_computation.3 | async-start | bytes 2097152 | tf_op jit(solution)/shard_map/all_to_all | solution.py:378
  84.6 14.7 %all-to-all-done.3 = bf16[16,16,2048]{2,1,0:T(8,128)(2,1)S(1)} async-done(((bf16[16,16,2048]{2,1,0:T(8,128)(2,1)}), bf16[16,16,2048]{2,1,0:T(8,128)(2,1)S(1)}, u32[]{:S(2)}, u32[]{:S(2)}) %all-to-all-start.3) | async-done | bytes 1048608 | tf_op jit(solution)/shard_map/all_to_all | solution.py:378
  99.3 4.7 %expert.1 = bf16[256,2048]{1,0:T(8,128)(2,1)S(1)} custom-call(bf16[256,2048]{1,0:T(8,128)(2,1)S(1)} %bitcast.46, bf16[2048,256]{1,0:T(8,128)(2,1)} %bitcast.18.g_ref, bf16[2048,256]{1,0:T(8,128)(2,1)} %bitcast.19.u_ref, bf16[256,2048]{1,0:T(8,128)(2,1)} %bitcast.20.d_ref, bf16[2048,256]{1,0:T(8,128)(2,1)} %collective-permute-done.4.pg_ref, ...), custom_call_target="tpu_custom_call" | custom-call | tf_op jit(solution)/shard_map/expert/pallas_call | solution.py:381
  104.0 17.3 %all_to_all.31 = bf16[16,16,2048]{2,1,0:T(8,128)(2,1)S(1)} all-to-all(bf16[16,16,2048]{2,1,0:T(8,128)(2,1)S(1)} %bitcast.47), channel_id=1, replica_groups=mesh['y'=4,'x'=4,'zh'=4,'zl'=2,'core'=2] {'y','x'}, dimensions={0} | all-to-all | bytes 2097152 | tf_op jit(solution)/shard_map/all_to_all | solution.py:387
  121.9 21.1 %all_to_all.32 = bf16[8,16,2048]{2,1,0:T(8,128)(2,1)S(1)} all-to-all(bf16[8,16,2048]{2,1,0:T(8,128)(2,1)S(1)} %bitcast.53), channel_id=1, replica_groups=mesh['y'=4,'x'=4,'zh'=4,'zl'=2,'core'=2] {'zh','zl'}, dimensions={0} | all-to-all | bytes 1048576 | tf_op jit(solution)/shard_map/all_to_all | solution.py:390
  143.0 0.6 add_convert_fusion
  (41 shorter events, 2.8 us)
Async XLA Ops:
  0.0 63.0 %copy-start = (bf16[512,2048]{1,0:T(8,128)(2,1)S(1)}, bf16[512,2048]{1,0:T(8,128)(2,1)}, u32[]{:S(2)}) copy-start(bf16[512,2048]{1,0:T(8,128)(2,1)} %param.45) | copy-start | bytes 6291460
  0.0 25.2 %collective-permute-start.1 = (bf16[128,2048]{1,0:T(8,128)(2,1)}, bf16[128,2048]{1,0:T(8,128)(2,1)S(1)}, u32[]{:S(2)}, u32[]{:S(2)}) collective-permute-start(bf16[128,2048]{1,0:T(8,128)(2,1)} %wv_ref.1), channel_id=1, source_target_pairs={{0,2},{2,0},{1,3},{3,1},{4,6},{6,4},{5,7},{7,5},{8,10},{10,8},{9,1... | collective-permute-start | bytes 1572872 | tf_op jit(solution)/shard_map/ppermute | solution.py:326
  2.5 22.8 %collective-permute-start.2 = (bf16[128,2048]{1,0:T(8,128)(2,1)}, bf16[128,2048]{1,0:T(8,128)(2,1)S(1)}, u32[]{:S(2)}, u32[]{:S(2)}) collective-permute-start(bf16[128,2048]{1,0:T(8,128)(2,1)} %wg_ref.1), channel_id=1, source_target_pairs={{0,2},{2,0},{1,3},{3,1},{4,6},{6,4},{5,7},{7,5},{8,10},{10,8},{9,1... | collective-permute-start | bytes 1572872 | tf_op jit(solution)/shard_map/ppermute | solution.py:326
  21.2 4.1 %collective-permute-start = (bf16[128,128]{1,0:T(8,128)(2,1)S(1)}, bf16[128,128]{1,0:T(8,128)(2,1)S(1)}, u32[]{:S(2)}, u32[]{:S(2)}) collective-permute-start(bf16[128,128]{1,0:T(8,128)(2,1)S(1)} %get-tuple-element.19), channel_id=1, source_target_pairs={{0,2},{2,0},{1,3},{3,1},{4,6},{6,4},{5,7},{7,5},{8,10},{10,8},{9,1... | collective-permute-start | bytes 98312 | tf_op jit(solution)/shard_map/ppermute | solution.py:326
  25.2 16.2 %copy-start.3 = (s32[256,2]{0,1:T(2,128)S(1)}, s32[256,2]{0,1:T(2,128)}, u32[]{:S(2)}) copy-start(s32[256,2]{0,1:T(2,128)} %param.38) | copy-start | bytes 6148
  25.2 16.5 %copy-start.4 = (f32[256,2]{0,1:T(2,128)S(1)}, f32[256,2]{0,1:T(2,128)}, u32[]{:S(2)}) copy-start(f32[256,2]{0,1:T(2,128)} %param.39) | copy-start | bytes 6148
  25.2 29.4 %copy-start.1 = (bf16[16,2048]{1,0:T(8,128)(2,1)S(1)}, bf16[16,2048]{1,0:T(8,128)(2,1)}, u32[]{:S(2)}) copy-start(bf16[16,2048]{1,0:T(8,128)(2,1)} %res_ref.1) | copy-start | bytes 196612
  25.2 29.3 %copy-start.2 = (f32[2048]{0:T(1024)S(1)}, f32[2048]{0:T(1024)}, u32[]{:S(2)}) copy-start(f32[2048]{0:T(1024)} %param.37) | copy-start | bytes 24580
  28.0 4.1 %collective-permute-start.3 = (bf16[4,16,4096]{2,1,0:T(8,128)(2,1)}, bf16[4,16,4096]{2,1,0:T(8,128)(2,1)S(1)}, u32[]{:S(2)}, u32[]{:S(2)}) collective-permute-start(bf16[4,16,4096]{2,1,0:T(8,128)(2,1)} %get-tuple-element.21), channel_id=1, source_target_pairs={{0,1},{1,0},{2,3},{3,2},{4,5},{5,4},{6,7},{7,6},{8,9},{9,8},{10,11... | collective-permute-start | bytes 1572872 | tf_op jit(solution)/shard_map/ppermute | solution.py:325
  30.4 54.2 %collective-permute-start.4 = (bf16[2048,256]{1,0:T(8,128)(2,1)}, bf16[2048,256]{1,0:T(8,128)(2,1)}, u32[]{:S(2)}, u32[]{:S(2)}) collective-permute-start(bf16[2048,256]{1,0:T(8,128)(2,1)} %bitcast.18.g_ref), channel_id=1, source_target_pairs={{0,1},{1,0},{2,3},{3,2},{4,5},{5,4},{6,7},{7,6},{8,9},{9,8},{10,11... | collective-permute-start | bytes 3145736 | tf_op jit(solution)/shard_map/ppermute | solution.py:325
  30.4 54.2 %collective-permute-start.5 = (bf16[2048,256]{1,0:T(8,128)(2,1)}, bf16[2048,256]{1,0:T(8,128)(2,1)}, u32[]{:S(2)}, u32[]{:S(2)}) collective-permute-start(bf16[2048,256]{1,0:T(8,128)(2,1)} %bitcast.19.u_ref), channel_id=1, source_target_pairs={{0,1},{1,0},{2,3},{3,2},{4,5},{5,4},{6,7},{7,6},{8,9},{9,8},{10,11... | collective-permute-start | bytes 3145736 | tf_op jit(solution)/shard_map/ppermute | solution.py:325
  30.9 53.7 %collective-permute-start.6 = (bf16[256,2048]{1,0:T(8,128)(2,1)}, bf16[256,2048]{1,0:T(8,128)(2,1)}, u32[]{:S(2)}, u32[]{:S(2)}) collective-permute-start(bf16[256,2048]{1,0:T(8,128)(2,1)} %bitcast.20.d_ref), channel_id=1, source_target_pairs={{0,1},{1,0},{2,3},{3,2},{4,5},{5,4},{6,7},{7,6},{8,9},{9,8},{10,11... | collective-permute-start | bytes 3145736 | tf_op jit(solution)/shard_map/ppermute | solution.py:325
  33.1 21.5 %all-to-all-start.1 = ((bf16[4,16,4096]{2,1,0:T(8,128)(2,1)}), bf16[4,16,4096]{2,1,0:T(8,128)(2,1)S(1)}, u32[]{:S(2)}, u32[]{:S(2)}) async-start(bf16[4,16,4096]{2,1,0:T(8,128)(2,1)} %shard_map.218), calls=%async_computation.1 | async-start | bytes 1048576 | tf_op jit(solution)/shard_map/all_to_all | solution.py:343
  55.6 21.1 %all-to-all-start.2 = ((bf16[8,16,2048]{2,1,0:T(8,128)(2,1)}), bf16[8,16,2048]{2,1,0:T(8,128)(2,1)S(1)}, u32[]{:S(2)}, u32[]{:S(2)}) async-start(bf16[8,16,2048]{2,1,0:T(8,128)(2,1)} %get-tuple-element.22), calls=%async_computation.2 | async-start | bytes 1048576 | tf_op jit(solution)/shard_map/all_to_all | solution.py:371
  78.2 21.1 %all-to-all-start.3 = ((bf16[16,16,2048]{2,1,0:T(8,128)(2,1)}), bf16[16,16,2048]{2,1,0:T(8,128)(2,1)S(1)}, u32[]{:S(2)}, u32[]{:S(2)}) async-start(bf16[16,16,2048]{2,1,0:T(8,128)(2,1)} %bitcast.51), calls=%async_computation.3 | async-start | bytes 2097152 | tf_op jit(solution)/shard_map/all_to_all | solution.py:378

commit v4 on v3

--- a/solution.py
+++ b/solution.py
@@ -305,11 +305,40 @@
     every_ref[...] = jnp.broadcast_to(normed[None], every_ref.shape)
 
 
-def expert_kernel(rows_ref, g_ref, u_ref, d_ref, pg_ref, pu_ref, pd_ref, out_ref):
+def shared_kernel(normed_ref, hidden_ref, g_ref, u_ref, d_ref, out_ref):
+    normed = normed_ref[...]
+    inner = (jax.nn.silu(dot(normed, g_ref[...])) * dot(normed, u_ref[...])).astype(BF16)
+    out_ref[...] = hidden_ref[...] + dot(inner, d_ref[...])
+
+
+def inner_kernel(rows_ref, g_ref, u_ref, pg_ref, pu_ref, keep_ref, send_ref):
     rows = rows_ref[...]
-    inner = (jax.nn.silu(dot(rows, g_ref[...])) * dot(rows, u_ref[...])).astype(BF16)
-    pair = (jax.nn.silu(dot(rows, pg_ref[...])) * dot(rows, pu_ref[...])).astype(BF16)
-    out_ref[...] = (dot(inner, d_ref[...]) + dot(pair, pd_ref[...])).astype(BF16)
+    width = g_ref.shape[1]
+    near = lax.axis_size("zh")
+    count, block = rows.shape[0] // 2, 2 * near
+    first = lax.axis_index("zl") == 0
+    square = (rows.shape[0], rows.shape[0])
+    out = lax.broadcasted_iota(jnp.int32, square, 0)
+    turn = out // count
+    source, rest = (out % count) // block, out % block
+    side = jnp.where(first, turn, 1 - turn)
+    place = source * 2 * block + (rest // 2) * 4 + side * 2 + rest % 2
+    order = jnp.where(lax.broadcasted_iota(jnp.int32, square, 1) == place, 1.0, 0.0)
+    order = order.astype(BF16)
+    for k, (gate_ref, up_ref) in enumerate(((g_ref, u_ref), (pg_ref, pu_ref))):
+        at = slice(k * width, (k + 1) * width)
+        inner = jax.nn.silu(dot(rows, gate_ref[...])) * dot(rows, up_ref[...])
+        moved = dot(order, inner.astype(BF16)).astype(BF16)
+        keep_ref[:, at] = moved[:count]
+        send_ref[:, at] = moved[count:]
+
+
+def down_kernel(keep_ref, got_ref, d_ref, pd_ref, fd_ref, fpd_ref, out_ref):
+    width = d_ref.shape[0]
+    kept, got = keep_ref[...], got_ref[...]
+    total = dot(kept[:, :width], d_ref[...]) + dot(kept[:, width:], pd_ref[...])
+    total = total + dot(got[:, :width], fd_ref[...]) + dot(got[:, width:], fpd_ref[...])
+    out_ref[...] = total.astype(BF16)
 
 
 def on_device(
@@ -320,7 +349,6 @@
     tok_loc, model_width = residual.shape
     layers = lax.axis_size(Z)
     owners = lax.axis_size(SP)
-    core = lax.axis_index("core")
     top_k = route_ids.shape[1]
     swap = lambda x: lax.ppermute(x, "core", [(0, 1), (1, 0)])
     cross = lambda x: lax.ppermute(x, "zl", [(0, 1), (1, 0)])
@@ -329,6 +357,7 @@
     gate_w, up_w, down_w = exp_gate[0], exp_up[0], exp_down[0]
     pair_eg, pair_eu, pair_ed = swap(gate_w), swap(up_w), swap(down_w)
 
+    corner = 2 * lax.axis_index("zl") + lax.axis_index("core")
     act_own, act_other = state_mixer(
         mixer_in, doc_ids, lam_re, lam_im, log_step, log_keep, in_re, in_im, out_re, out_im,
         skip_gain,
@@ -341,6 +370,34 @@
     )
     parts = call(sum_kernel, shape, kept, swap(sent))
     parts = lax.all_to_all(parts, "zh", 0, 0, tiled=True)
+    capacity = tok_loc * top_k // owners
+
+    def placed(ids, wts, count):
+        ids = ids.reshape(count, tok_loc * top_k)
+        same = ids[:, :, None] == ids[:, None, :]
+        order = jnp.arange(tok_loc * top_k)
+        rank = jnp.sum((same & (order[None, :] < order[:, None])).astype(jnp.int32), axis=-1)
+        block = count * capacity
+        slots = ids * block + capacity * jnp.arange(count, dtype=jnp.int32)[:, None] + rank
+        slots = slots.reshape(count * tok_loc, top_k)
+        hit = slots[:, :, None] == jnp.arange(owners * block, dtype=jnp.int32)[None, None, :]
+        if wts is None:
+            return jnp.sum(hit.astype(F32), axis=1).astype(BF16)
+        wts = wts.reshape(count * tok_loc, top_k)
+        return halves(jnp.sum(jnp.where(hit, wts[:, :, None], 0.0), axis=1))
+
+    def mine(x, count, parts, at):
+        x = x.reshape(count, parts, tok_loc, top_k)
+        return lax.dynamic_index_in_dim(x, at, 1, keepdims=False)
+
+    block = layers * capacity
+    picker = placed(mine(route_ids, layers, 2, lax.axis_index("core")), None, layers)
+    weights_high, weights_low = placed(
+        mine(route_ids, near, 4, corner), mine(route_wts, near, 4, corner), near
+    )
+    parts, picker, weights_high, weights_low = lax.optimization_barrier(
+        (parts, picker, weights_high, weights_low)
+    )
     every, hidden, normed = call(
         norm_kernel,
         (
@@ -352,42 +409,34 @@
     )
 
     tokens = layers * tok_loc
-    mine = lambda x: lax.dynamic_index_in_dim(
-        x.reshape(layers, 2, tok_loc, top_k), core, 1, keepdims=False
-    )
-    ids = mine(route_ids).reshape(layers, tok_loc * top_k)
-    wts = mine(route_wts).reshape(tokens, top_k)
-    same = ids[:, :, None] == ids[:, None, :]
-    order = jnp.arange(tok_loc * top_k)
-    rank = jnp.sum((same & (order[None, :] < order[:, None])).astype(jnp.int32), axis=-1)
-    capacity = tok_loc * top_k // owners
-    block = layers * capacity
-    slots = ids * block + capacity * jnp.arange(layers, dtype=jnp.int32)[:, None] + rank
-    slots = slots.reshape(tokens, top_k)
-    hit = slots[:, :, None] == jnp.arange(owners * block, dtype=jnp.int32)[None, None, :]
-    picker = jnp.sum(hit.astype(F32), axis=1).astype(BF16)
-    weights_high, weights_low = halves(jnp.sum(jnp.where(hit, wts[:, :, None], 0.0), axis=1))
-
     every = lax.all_to_all(every, Z, 0, 0, tiled=True).reshape(tokens, model_width)
-    shared_inner = (jax.nn.silu(dot(normed, shared_gate)) * dot(normed, shared_up)).astype(BF16)
-    base = hidden + dot(shared_inner, shared_down)
-    every, base = lax.optimization_barrier((every, base))
+    base = call(
+        shared_kernel, jax.ShapeDtypeStruct(hidden.shape, F32),
+        normed, hidden, *map(in_hbm, (shared_gate, shared_up, shared_down)),
+    )
+    every, base, down_now = lax.optimization_barrier((every, base, down_w))
+    far_down = cross(down_now)
+    far_pair = swap(far_down)
     packed = lax.dot_general(
         picker, every, (((0,), (0,)), ((), ())), preferred_element_type=F32
     ).astype(BF16)
     rows = lax.all_to_all(packed.reshape(owners, block, model_width), SP, 0, 0, tiled=True)
     rows = rows.reshape(owners * block, model_width)
-    operands = (rows, gate_w, up_w, down_w, pair_eg, pair_eu, pair_ed)
-    partial = pl.pallas_call(
-        expert_kernel,
-        out_shape=jax.ShapeDtypeStruct(rows.shape, BF16),
-        name="expert",
-        compiler_params=SMALL,
-    )(*operands)
-    back = lax.all_to_all(partial.reshape(owners, block, model_width), SP, 0, 0, tiled=True)
-    back = back.reshape(owners * block, model_width)
+    half = owners * block // 2
+    narrow = jax.ShapeDtypeStruct((half, 2 * gate_w.shape[1]), BF16)
+    kept, sent = call(
+        inner_kernel, (narrow, narrow), rows, *map(in_hbm, (gate_w, up_w, pair_eg, pair_eu)),
+    )
+    partial = call(
+        down_kernel,
+        jax.ShapeDtypeStruct((half, model_width), BF16),
+        kept, cross(sent), in_hbm(down_w), in_hbm(pair_ed), far_down, far_pair,
+    )
+    back = lax.all_to_all(
+        partial.reshape(owners, block // 2, model_width), SP, 0, 0, tiled=True
+    ).reshape(half, model_width)
     routed = (dot(weights_high, back) + dot(weights_low, back)).astype(BF16)
-    routed = lax.all_to_all(routed.reshape(layers, tok_loc, model_width), Z, 0, 0, tiled=True)
+    routed = lax.all_to_all(routed.reshape(near, tok_loc, model_width), "zh", 0, 0, tiled=True)
     return (base + jnp.sum(routed.astype(F32), axis=0)).astype(BF16)
 
 

time: 145 us -> 152 us (1.048)
  blocking collectives: 51.7 us -> 27 us
  starting transfers between devices: 26.6 us -> 41.9 us
  waiting for transfers between devices: 42 us -> 54.1 us
  Pallas kernels: 14.7 us -> 19.6 us
  matrix products: 6.37 us -> 1.89 us
  local copies, waits for them, and re-layouts: 0.89 us -> 3.61 us
    all_to_all x3 -> x2, blocking collectives: 51.7 us -> 27 us  [the longest x1 15.4 us: on_device(): lax.all_to_all(partial.reshape(owners, block // 2, model_width), SP, 0, 0...]
    ppermute x3 -> x5, waiting for transfers between devices: 2.6 us -> 23.6 us  [on_device(): cross = lambda x: lax.ppermute(x, 'zl', [(0, 1), (1, 0)])]
    all_to_all x1, waiting for transfers between devices: 14.7 us -> 1.96 us  [on_device(): lax.all_to_all(packed.reshape(owners, block, model_width), SP, 0, 0, tile...]
    pallas_call x3 -> x6, Pallas kernels: 4.74 us -> 13.8 us  [call(): pl.pallas_call(kernel, out_shape=outs, compiler_params=SMALL)(*operands)]
    all_to_all x0 -> x1, starting transfers between devices: none -> 7.59 us  [state_mixer(): got = lax.all_to_all(send, SP, 0, 0, tiled=True)]
    ppermute x4 -> x5, starting transfers between devices: 2.86 us -> 9.98 us  [on_device(): swap = lambda x: lax.ppermute(x, 'core', [(0, 1), (1, 0)])]
    pallas_call x1 -> x0, Pallas kernels: 4.71 us -> none  [on_device(): pl.pallas_call(expert_kernel, out_shape=jax.ShapeDtypeStruct(rows.shape,...]
    dot_general x4 -> x2, matrix products: 4.92 us -> 0.44 us  [dot(): return jnp.dot(a, b, preferred_element_type=F32)]
  transfers between devices with their start and end apart: 10 -> 14, of which waited for: 5 -> 8; matrix products, arithmetic and copies ran while one was open for 5% -> 4% of each run, Pallas kernels for 5% -> 7%
where the time goes in v4:
time: 152 us; the launch traced here: 150 us
  waiting for transfers between devices  54.1 us (36%)
  starting transfers between devices  41.9 us (28%)
  blocking collectives  27 us (18%)
  Pallas kernels  19.6 us (13%)
  local copies, waits for them, and re-layouts  3.61 us (2%)
  matrix products  1.89 us (1%)
  other arithmetic  1.52 us (1%)
    ppermute x5, waiting for transfers between devices, on_device(): cross = lambda x: lax.ppermute(x, 'zl', [(0, 1), (1, 0)])  23.6 us
    all_to_all x1, blocking collectives, on_device(): lax.all_to_all(partial.reshape(owners, block // 2, model_width), SP, 0, 0...  15.4 us
    pallas_call x6, Pallas kernels, call(): pl.pallas_call(kernel, out_shape=outs, compiler_params=SMALL)(*operands)  13.8 us
    all_to_all x1, waiting for transfers between devices, on_device(): parts = lax.all_to_all(parts, 'zh', 0, 0, tiled=True)  12.8 us
    all_to_all x1, waiting for transfers between devices, on_device(): lax.all_to_all(every, Z, 0, 0, tiled=True).reshape(tokens, model_width)  11.7 us
    all_to_all x1, blocking collectives, on_device(): lax.all_to_all(routed.reshape(near, tok_loc, model_width), 'zh', 0, 0, ti...  11.6 us
    ppermute x5, starting transfers between devices, on_device(): swap = lambda x: lax.ppermute(x, 'core', [(0, 1), (1, 0)])  9.98 us
    all_to_all x1, starting transfers between devices, on_device(): parts = lax.all_to_all(parts, 'zh', 0, 0, tiled=True)  7.99 us
  transfers between devices with their start and end apart: 14, of which 8 were waited for; matrix products, arithmetic and copies ran while one was open for 4% of the time, Pallas kernels for 7%

profile of v4, /device:TPU:1, one launch (start us, length us, event | category | flops | bytes accessed | tf_op | source)
XLA Modules:
  0.0 149.8 jit_solution(11236815889557367287)
XLA Ops:
  0.0 2.5 %drive.1 = (f32[16,4,512]{2,1,0:T(4,128)}, f32[3,8,512]{2,1,0:T(8,128)S(1)}) custom-call(bf16[256,128]{1,0:T(8,128)(2,1)} %refs_0_.3, f32[8,256]{1,0:T(8,128)} %bitcast.66, s32[1,256]{1,0:T(1,128)} %bitcast.69, f32[8,64]{1,0:T(8,128)} %refs_3_.3, f32[8,64]{1,0:T(8,128)} %refs_4_.3, f32[1,8]{1,0:T(1,128)} %bitcast.71, f32[128,64]{1,0:T(8,128)} %bitcast.54, ...), custom_call_target="tpu_custom_call" | custom-call | tf_op jit(solution)/shard_map/drive/pallas_call | solution.py:255
  2.5 7.6 %all-to-all-start = ((f32[16,4,512]{2,1,0:T(4,128)}), f32[16,4,512]{2,1,0:T(4,128)S(1)}, u32[]{:S(2)}, u32[]{:S(2)}) async-start(f32[16,4,512]{2,1,0:T(4,128)} %get-tuple-element.23), calls=%async_computation | async-start | bytes 262144 | tf_op jit(solution)/shard_map/all_to_all | solution.py:265
  10.2 1.7 %collective-permute-start.1 = (bf16[128,2048]{1,0:T(8,128)(2,1)}, bf16[128,2048]{1,0:T(8,128)(2,1)S(1)}, u32[]{:S(2)}, u32[]{:S(2)}) collective-permute-start(bf16[128,2048]{1,0:T(8,128)(2,1)} %wv_ref.1), channel_id=1, source_target_pairs={{0,2},{2,0},{1,3},{3,1},{4,6},{6,4},{5,7},{7,5},{8,10},{10,8},{9,1... | collective-permute-start | bytes 1572872 | tf_op jit(solution)/shard_map/ppermute | solution.py:354
  13.6 3.4 %all-to-all-done.refs_8_ = f32[16,4,512]{2,1,0:T(4,128)S(1)} async-done(((f32[16,4,512]{2,1,0:T(4,128)}), f32[16,4,512]{2,1,0:T(4,128)S(1)}, u32[]{:S(2)}, u32[]{:S(2)}) %all-to-all-start) | async-done | bytes 131104 | tf_op jit(solution)/shard_map/all_to_all | solution.py:265
  17.0 3.3 %readout.1 = (bf16[128,128]{1,0:T(8,128)(2,1)S(1)}, bf16[128,128]{1,0:T(8,128)(2,1)S(1)}) custom-call(bf16[256,128]{1,0:T(8,128)(2,1)} %refs_0_.3, f32[8,256]{1,0:T(8,128)} %bitcast.67, s32[1,256]{1,0:T(1,128)} %bitcast.70, f32[8,64]{1,0:T(8,128)} %refs_3_.3, f32[8,64]{1,0:T(8,128)} %refs_4_.3, f32[1,8]{1,0:T(1,128)} %bitcast.72, f32[128,64]{1,0:T(8,128)} %bitcast.55, ...), custom_call_target="tpu_custom_call" | custom-call | tf_op jit(solution)/shard_map/readout/pallas_call | solution.py:267
  20.3 1.7 %collective-permute-start = (bf16[128,128]{1,0:T(8,128)(2,1)S(1)}, bf16[128,128]{1,0:T(8,128)(2,1)S(1)}, u32[]{:S(2)}, u32[]{:S(2)}) collective-permute-start(bf16[128,128]{1,0:T(8,128)(2,1)S(1)} %get-tuple-element.26), channel_id=1, source_target_pairs={{0,2},{2,0},{1,3},{3,1},{4,6},{6,4},{5,7},{7,5},{8,10},{10,8},{9,1... | collective-permute-start | bytes 98312 | tf_op jit(solution)/shard_map/ppermute | solution.py:354
  23.7 11.5 %collective-permute-done.pair_ref = bf16[128,128]{1,0:T(8,128)(2,1)S(1)} collective-permute-done((bf16[128,128]{1,0:T(8,128)(2,1)S(1)}, bf16[128,128]{1,0:T(8,128)(2,1)S(1)}, u32[]{:S(2)}, u32[]{:S(2)}) %collective-permute-start) | collective-permute-done | bytes 32800 | tf_op jit(solution)/shard_map/ppermute | solution.py:354
  35.3 1.9 %shard_map.217 = (bf16[4,16,4096]{2,1,0:T(8,128)(2,1)S(1)}, bf16[4,16,4096]{2,1,0:T(8,128)(2,1)S(1)}) custom-call(bf16[128,128]{1,0:T(8,128)(2,1)S(1)} %get-tuple-element.25.own_ref, bf16[128,128]{1,0:T(8,128)(2,1)S(1)} %collective-permute-done.pair_ref, bf16[128,2048]{1,0:T(8,128)(2,1)} %wv_ref.1, bf16[128,2048]{1,0:T(8,128)(2,1)} %wg_ref.1, ...), custom_call_target="tpu_custom_call" | custom-call | tf_op jit(solution)/shard_map/pallas_call | solution.py:31
  37.2 1.7 %collective-permute-start.3 = (bf16[4,16,4096]{2,1,0:T(8,128)(2,1)S(1)}, bf16[4,16,4096]{2,1,0:T(8,128)(2,1)S(1)}, u32[]{:S(2)}, u32[]{:S(2)}) collective-permute-start(bf16[4,16,4096]{2,1,0:T(8,128)(2,1)S(1)} %get-tuple-element.28), channel_id=1, source_target_pairs={{0,1},{1,0},{2,3},{3,2},{4,5},{5,4},{6,7},{7,6},{8,9},{9,8},{10,11... | collective-permute-start | bytes 1572872 | tf_op jit(solution)/shard_map/ppermute | solution.py:353
  41.4 8.0 %all-to-all-start.1 = ((bf16[4,16,4096]{2,1,0:T(8,128)(2,1)}), bf16[4,16,4096]{2,1,0:T(8,128)(2,1)S(1)}, u32[]{:S(2)}, u32[]{:S(2)}) async-start(bf16[4,16,4096]{2,1,0:T(8,128)(2,1)} %shard_map.218), calls=%async_computation.1 | async-start | bytes 1048576 | tf_op jit(solution)/shard_map/all_to_all | solution.py:372
  49.8 12.8 %all-to-all-done.1.parts_ref = bf16[4,16,4096]{2,1,0:T(8,128)(2,1)S(1)} async-done(((bf16[4,16,4096]{2,1,0:T(8,128)(2,1)}), bf16[4,16,4096]{2,1,0:T(8,128)(2,1)S(1)}, u32[]{:S(2)}, u32[]{:S(2)}) %all-to-all-start.1) | async-done | bytes 524320 | tf_op jit(solution)/shard_map/all_to_all | solution.py:372
  63.6 4.9 %all-to-all-start.2 = ((bf16[8,16,2048]{2,1,0:T(8,128)(2,1)}), bf16[8,16,2048]{2,1,0:T(8,128)(2,1)S(1)}, u32[]{:S(2)}, u32[]{:S(2)}) async-start(bf16[8,16,2048]{2,1,0:T(8,128)(2,1)} %get-tuple-element.30), calls=%async_computation.2 | async-start | bytes 1048576 | tf_op jit(solution)/shard_map/all_to_all | solution.py:412
  68.4 3.9 %shard_map.220 = f32[16,2048]{1,0:T(8,128)S(1)} custom-call(bf16[16,2048]{1,0:T(8,128)(2,1)S(1)} %get-tuple-element.31.normed_ref, f32[16,2048]{1,0:T(8,128)S(1)} %get-tuple-element.32.hidden_ref, bf16[2048,512]{1,0:T(8,128)(2,1)} %g_ref.1, bf16[2048,512]{1,0:T(8,128)(2,1)} %u_ref.1, bf16[512,2048]{1,0:T(8,128)(2,1)} %d_ref.1), custom_call_target="tpu_custom_call" | custom-call | tf_op jit(solution)/shard_map/pallas_call | solution.py:31
  72.3 11.7 %all-to-all-done.2 = bf16[8,16,2048]{2,1,0:T(8,128)(2,1)S(1)} async-done(((bf16[8,16,2048]{2,1,0:T(8,128)(2,1)}), bf16[8,16,2048]{2,1,0:T(8,128)(2,1)S(1)}, u32[]{:S(2)}, u32[]{:S(2)}) %all-to-all-start.2) | async-done | bytes 524320 | tf_op jit(solution)/shard_map/all_to_all | solution.py:412
  84.0 3.5 %collective-permute-start.4 = (bf16[2048,256]{1,0:T(8,128)(2,1)}, bf16[2048,256]{1,0:T(8,128)(2,1)}, u32[]{:S(2)}, u32[]{:S(2)}) collective-permute-start(bf16[2048,256]{1,0:T(8,128)(2,1)} %bitcast.20.g_ref), channel_id=1, source_target_pairs={{0,1},{1,0},{2,3},{3,2},{4,5},{5,4},{6,7},{7,6},{8,9},{9,8},{10,11... | collective-permute-start | bytes 3145736 | tf_op jit(solution)/shard_map/ppermute | solution.py:353
  88.9 6.6 %all-to-all-start.3 = ((bf16[16,16,2048]{2,1,0:T(8,128)(2,1)}), bf16[16,16,2048]{2,1,0:T(8,128)(2,1)S(1)}, u32[]{:S(2)}, u32[]{:S(2)}) async-start(bf16[16,16,2048]{2,1,0:T(8,128)(2,1)} %bitcast.18), calls=%async_computation.3 | async-start | bytes 2097152 | tf_op jit(solution)/shard_map/all_to_all | solution.py:423
  96.4 9.5 %collective-permute-done.8.fd_ref = bf16[256,2048]{1,0:T(8,128)(2,1)S(1)} collective-permute-done((bf16[256,2048]{1,0:T(8,128)(2,1)}, bf16[256,2048]{1,0:T(8,128)(2,1)S(1)}, u32[]{:S(2)}, u32[]{:S(2)}) %collective-permute-start.8) | collective-permute-done | bytes 1048608 | tf_op jit(solution)/shard_map/ppermute | solution.py:354
  105.9 3.9 %collective-permute-start.9 = (bf16[256,2048]{1,0:T(8,128)(2,1)S(1)}, bf16[256,2048]{1,0:T(8,128)(2,1)S(1)}, u32[]{:S(2)}, u32[]{:S(2)}) collective-permute-start(bf16[256,2048]{1,0:T(8,128)(2,1)S(1)} %collective-permute-done.8.fd_ref), channel_id=1, source_target_pairs={{0,1},{1,0},{2,3},{3,2},{4,5},{5,4},{6,7},{7,6},{8,9},{9,8},{10,11... | collective-permute-start | bytes 3145736 | tf_op jit(solution)/shard_map/ppermute | solution.py:353
  109.8 2.0 %all-to-all-done.3 = bf16[16,16,2048]{2,1,0:T(8,128)(2,1)S(1)} async-done(((bf16[16,16,2048]{2,1,0:T(8,128)(2,1)}), bf16[16,16,2048]{2,1,0:T(8,128)(2,1)S(1)}, u32[]{:S(2)}, u32[]{:S(2)}) %all-to-all-start.3) | async-done | bytes 1048608 | tf_op jit(solution)/shard_map/all_to_all | solution.py:423
  111.7 3.8 %shard_map.221 = (bf16[128,512]{1,0:T(8,128)(2,1)S(1)}, bf16[128,512]{1,0:T(8,128)(2,1)S(1)}) custom-call(bf16[256,2048]{1,0:T(8,128)(2,1)S(1)} %bitcast.49, bf16[2048,256]{1,0:T(8,128)(2,1)} %bitcast.20.g_ref, bf16[2048,256]{1,0:T(8,128)(2,1)} %bitcast.21.u_ref, bf16[2048,256]{1,0:T(8,128)(2,1)} %collective-permute-done.4.pg_ref, ...), custom_call_target="tpu_custom_call" | custom-call | tf_op jit(solution)/shard_map/pallas_call | solution.py:31
  116.9 2.5 %collective-permute-done.6.got_ref = bf16[128,512]{1,0:T(8,128)(2,1)S(1)} collective-permute-done((bf16[128,512]{1,0:T(8,128)(2,1)S(1)}, bf16[128,512]{1,0:T(8,128)(2,1)S(1)}, u32[]{:S(2)}, u32[]{:S(2)}) %collective-permute-start.6) | collective-permute-done | bytes 131104 | tf_op jit(solution)/shard_map/ppermute | solution.py:354
  119.5 2.3 %shard_map.222 = bf16[128,2048]{1,0:T(8,128)(2,1)S(1)} custom-call(bf16[128,512]{1,0:T(8,128)(2,1)S(1)} %get-tuple-element.37.keep_ref, bf16[128,512]{1,0:T(8,128)(2,1)S(1)} %collective-permute-done.6.got_ref, bf16[256,2048]{1,0:T(8,128)(2,1)} %bitcast.17.d_ref, bf16[256,2048]{1,0:T(8,128)(2,1)} %collective-permute-done.7.pd_ref, ...), custom_call_target="tpu_custom_call" | custom-call | tf_op jit(solution)/shard_map/pallas_call | solution.py:31
  121.7 15.4 %all_to_all.30 = bf16[16,8,2048]{2,1,0:T(8,128)(2,1)S(1)} all-to-all(bf16[16,8,2048]{2,1,0:T(8,128)(2,1)S(1)} %bitcast.50), channel_id=1, replica_groups=mesh['y'=4,'x'=4,'zh'=4,'zl'=2,'core'=2] {'y','x'}, dimensions={0} | all-to-all | bytes 1048576 | tf_op jit(solution)/shard_map/all_to_all | solution.py:435
  137.6 11.6 %all_to_all.31 = bf16[4,16,2048]{2,1,0:T(8,128)(2,1)S(1)} all-to-all(bf16[4,16,2048]{2,1,0:T(8,128)(2,1)S(1)} %bitcast.53), channel_id=1, replica_groups=mesh['y'=4,'x'=4,'zh'=4,'zl'=2,'core'=2] {'zh'}, dimensions={0} | all-to-all | bytes 524288 | tf_op jit(solution)/shard_map/all_to_all | solution.py:439
  (56 shorter events, 12.1 us)
Async XLA Ops:
  2.5 14.5 %all-to-all-start = ((f32[16,4,512]{2,1,0:T(4,128)}), f32[16,4,512]{2,1,0:T(4,128)S(1)}, u32[]{:S(2)}, u32[]{:S(2)}) async-start(f32[16,4,512]{2,1,0:T(4,128)} %get-tuple-element.23), calls=%async_computation | async-start | bytes 262144 | tf_op jit(solution)/shard_map/all_to_all | solution.py:265
  10.2 25.1 %collective-permute-start.1 = (bf16[128,2048]{1,0:T(8,128)(2,1)}, bf16[128,2048]{1,0:T(8,128)(2,1)S(1)}, u32[]{:S(2)}, u32[]{:S(2)}) collective-permute-start(bf16[128,2048]{1,0:T(8,128)(2,1)} %wv_ref.1), channel_id=1, source_target_pairs={{0,2},{2,0},{1,3},{3,1},{4,6},{6,4},{5,7},{7,5},{8,10},{10,8},{9,1... | collective-permute-start | bytes 1572872 | tf_op jit(solution)/shard_map/ppermute | solution.py:354
  11.9 23.4 %collective-permute-start.2 = (bf16[128,2048]{1,0:T(8,128)(2,1)}, bf16[128,2048]{1,0:T(8,128)(2,1)S(1)}, u32[]{:S(2)}, u32[]{:S(2)}) collective-permute-start(bf16[128,2048]{1,0:T(8,128)(2,1)} %wg_ref.1), channel_id=1, source_target_pairs={{0,2},{2,0},{1,3},{3,1},{4,6},{6,4},{5,7},{7,5},{8,10},{10,8},{9,1... | collective-permute-start | bytes 1572872 | tf_op jit(solution)/shard_map/ppermute | solution.py:354
  20.3 15.0 %collective-permute-start = (bf16[128,128]{1,0:T(8,128)(2,1)S(1)}, bf16[128,128]{1,0:T(8,128)(2,1)S(1)}, u32[]{:S(2)}, u32[]{:S(2)}) collective-permute-start(bf16[128,128]{1,0:T(8,128)(2,1)S(1)} %get-tuple-element.26), channel_id=1, source_target_pairs={{0,2},{2,0},{1,3},{3,1},{4,6},{6,4},{5,7},{7,5},{8,10},{10,8},{9,1... | collective-permute-start | bytes 98312 | tf_op jit(solution)/shard_map/ppermute | solution.py:354
  35.3 27.3 %copy-start = (bf16[16,2048]{1,0:T(8,128)(2,1)S(1)}, bf16[16,2048]{1,0:T(8,128)(2,1)}, u32[]{:S(2)}) copy-start(bf16[16,2048]{1,0:T(8,128)(2,1)} %res_ref.1) | copy-start | bytes 196612
  35.3 27.3 %copy-start.1 = (f32[2048]{0:T(1024)S(1)}, f32[2048]{0:T(1024)}, u32[]{:S(2)}) copy-start(f32[2048]{0:T(1024)} %param.37) | copy-start | bytes 24580
  37.2 3.3 %collective-permute-start.3 = (bf16[4,16,4096]{2,1,0:T(8,128)(2,1)S(1)}, bf16[4,16,4096]{2,1,0:T(8,128)(2,1)S(1)}, u32[]{:S(2)}, u32[]{:S(2)}) collective-permute-start(bf16[4,16,4096]{2,1,0:T(8,128)(2,1)S(1)} %get-tuple-element.28), channel_id=1, source_target_pairs={{0,1},{1,0},{2,3},{3,2},{4,5},{5,4},{6,7},{7,6},{8,9},{9,8},{10,11... | collective-permute-start | bytes 1572872 | tf_op jit(solution)/shard_map/ppermute | solution.py:353
  41.4 21.2 %all-to-all-start.1 = ((bf16[4,16,4096]{2,1,0:T(8,128)(2,1)}), bf16[4,16,4096]{2,1,0:T(8,128)(2,1)S(1)}, u32[]{:S(2)}, u32[]{:S(2)}) async-start(bf16[4,16,4096]{2,1,0:T(8,128)(2,1)} %shard_map.218), calls=%async_computation.1 | async-start | bytes 1048576 | tf_op jit(solution)/shard_map/all_to_all | solution.py:372
  63.6 20.4 %all-to-all-start.2 = ((bf16[8,16,2048]{2,1,0:T(8,128)(2,1)}), bf16[8,16,2048]{2,1,0:T(8,128)(2,1)S(1)}, u32[]{:S(2)}, u32[]{:S(2)}) async-start(bf16[8,16,2048]{2,1,0:T(8,128)(2,1)} %get-tuple-element.30), calls=%async_computation.2 | async-start | bytes 1048576 | tf_op jit(solution)/shard_map/all_to_all | solution.py:412
  84.0 21.9 %collective-permute-start.8 = (bf16[256,2048]{1,0:T(8,128)(2,1)}, bf16[256,2048]{1,0:T(8,128)(2,1)S(1)}, u32[]{:S(2)}, u32[]{:S(2)}) collective-permute-start(bf16[256,2048]{1,0:T(8,128)(2,1)} %bitcast.17.d_ref), channel_id=1, source_target_pairs={{0,2},{2,0},{1,3},{3,1},{4,6},{6,4},{5,7},{7,5},{8,10},{10,8},{9,1... | collective-permute-start | bytes 3145736 | tf_op jit(solution)/shard_map/ppermute | solution.py:354
  84.0 25.8 %collective-permute-start.4 = (bf16[2048,256]{1,0:T(8,128)(2,1)}, bf16[2048,256]{1,0:T(8,128)(2,1)}, u32[]{:S(2)}, u32[]{:S(2)}) collective-permute-start(bf16[2048,256]{1,0:T(8,128)(2,1)} %bitcast.20.g_ref), channel_id=1, source_target_pairs={{0,1},{1,0},{2,3},{3,2},{4,5},{5,4},{6,7},{7,6},{8,9},{9,8},{10,11... | collective-permute-start | bytes 3145736 | tf_op jit(solution)/shard_map/ppermute | solution.py:353
  87.5 22.3 %collective-permute-start.5 = (bf16[2048,256]{1,0:T(8,128)(2,1)}, bf16[2048,256]{1,0:T(8,128)(2,1)}, u32[]{:S(2)}, u32[]{:S(2)}) collective-permute-start(bf16[2048,256]{1,0:T(8,128)(2,1)} %bitcast.21.u_ref), channel_id=1, source_target_pairs={{0,1},{1,0},{2,3},{3,2},{4,5},{5,4},{6,7},{7,6},{8,9},{9,8},{10,11... | collective-permute-start | bytes 3145736 | tf_op jit(solution)/shard_map/ppermute | solution.py:353
  88.9 22.8 %all-to-all-start.3 = ((bf16[16,16,2048]{2,1,0:T(8,128)(2,1)}), bf16[16,16,2048]{2,1,0:T(8,128)(2,1)S(1)}, u32[]{:S(2)}, u32[]{:S(2)}) async-start(bf16[16,16,2048]{2,1,0:T(8,128)(2,1)} %bitcast.18), calls=%async_computation.3 | async-start | bytes 2097152 | tf_op jit(solution)/shard_map/all_to_all | solution.py:423
  95.5 21.4 %collective-permute-start.7 = (bf16[256,2048]{1,0:T(8,128)(2,1)}, bf16[256,2048]{1,0:T(8,128)(2,1)}, u32[]{:S(2)}, u32[]{:S(2)}) collective-permute-start(bf16[256,2048]{1,0:T(8,128)(2,1)} %bitcast.17.d_ref), channel_id=1, source_target_pairs={{0,1},{1,0},{2,3},{3,2},{4,5},{5,4},{6,7},{7,6},{8,9},{9,8},{10,11... | collective-permute-start | bytes 3145736 | tf_op jit(solution)/shard_map/ppermute | solution.py:353
  105.9 13.6 %collective-permute-start.9 = (bf16[256,2048]{1,0:T(8,128)(2,1)S(1)}, bf16[256,2048]{1,0:T(8,128)(2,1)S(1)}, u32[]{:S(2)}, u32[]{:S(2)}) collective-permute-start(bf16[256,2048]{1,0:T(8,128)(2,1)S(1)} %collective-permute-done.8.fd_ref), channel_id=1, source_target_pairs={{0,1},{1,0},{2,3},{3,2},{4,5},{5,4},{6,7},{7,6},{8,9},{9,8},{10,11... | collective-permute-start | bytes 3145736 | tf_op jit(solution)/shard_map/ppermute | solution.py:353
  115.5 3.9 %collective-permute-start.6 = (bf16[128,512]{1,0:T(8,128)(2,1)S(1)}, bf16[128,512]{1,0:T(8,128)(2,1)S(1)}, u32[]{:S(2)}, u32[]{:S(2)}) collective-permute-start(bf16[128,512]{1,0:T(8,128)(2,1)S(1)} %get-tuple-element.38), channel_id=1, source_target_pairs={{0,2},{2,0},{1,3},{3,1},{4,6},{6,4},{5,7},{7,5},{8,10},{10,8},{9,1... | collective-permute-start | bytes 393224 | tf_op jit(solution)/shard_map/ppermute | solution.py:354
